TPU v7x, 128 devices: a whole 4x4x4 slice. The times are simulated.
128 devices in a mesh: sp: 16 (over z, x), dp: 8 (over y, core).
Axes of the slice: x: 4, y: 4, z: 4, core: 2. Of those that a mesh axis runs over, the one named last changes fastest.
Arguments:
- hidden_in: bfloat16 [8, 2048, 2048], P('dp', 'sp'), may hold values from -6 to 6
- mix_cotangent: bfloat16 [8, 2048, 4096], P('dp', 'sp'), may hold values from -0.119628906 to 0.119628906
- query_weight: bfloat16 [2048, 4096], P('dp', 'sp'), may hold values from -0.125 to 0.125
- key_weight: bfloat16 [2048, 4096], P('dp', 'sp'), may hold values from -0.125 to 0.125
- value_weight: bfloat16 [2048, 4096], P('dp', 'sp'), may hold values from -0.125 to 0.125
- decay_log: float32 [16], P('sp'), may hold values from -0.034 to -0.000146484375, as said below
Outputs:
- grad_hidden: bfloat16 [8, 2048, 2048], P('dp', 'sp')
- grad_query: float32 [2048, 4096], P('dp', 'sp')
- grad_key: float32 [2048, 4096], P('dp', 'sp')
- grad_value: float32 [2048, 4096], P('dp', 'sp')
Inputs may be any that keep to these rules, and one draw needn't show every extreme that they name: Each head's decay_log is negative.
All inputs are finite; a program needn't handle non-finite values.
Results may differ from a plain program's by a relative error of at most 0.015.
Values may be sent and summed in bfloat16 or wider, within the bound.
A program may use at most 64 MiB of HBM per device.

v0:
```python
import jax
import jax.numpy as jnp
from jax import lax
from jax.sharding import PartitionSpec as P

BLOCK = 128


def in_blocks(array, dim, size):
    shape = array.shape
    pieces = array.reshape(*shape[:dim], size, shape[dim] // size, *shape[dim + 1 :])
    return jnp.moveaxis(pieces, dim, 0)


def sent_and_summed(array, axis, dim):
    pieces = in_blocks(array, dim, lax.axis_size(axis))
    arrived = lax.all_to_all(pieces, axis, split_axis=0, concat_axis=0, tiled=True)
    return arrived.astype(jnp.float32).sum(axis=0)


def head_grads(queries, key_rows, values, cotangent, log_rate):
    length = queries.shape[0]
    head_dim = queries.shape[1]
    blocks = length // BLOCK
    scale = head_dim ** (-0.5)
    keys_scaled = (key_rows.astype(jnp.float32) * scale).astype(jnp.bfloat16)
    offsets = jnp.arange(BLOCK, dtype=jnp.float32)
    spread = offsets[:, None] - offsets[None, :]
    inner_decay = jnp.where(spread >= 0, jnp.exp(log_rate * jnp.maximum(spread, 0.0)), 0.0)
    query_decay = jnp.exp(log_rate * (offsets + 1.0))
    key_decay = jnp.exp(log_rate * (BLOCK - 1.0 - offsets))
    block_decay = jnp.exp(log_rate * BLOCK)

    def split_blocks(series):
        return series.reshape(blocks, BLOCK, series.shape[-1])

    def forward(carried, inputs):
        query_block, key_block, value_block, grad_block = inputs
        mixed = (
            jnp.dot(grad_block, value_block.T, preferred_element_type=jnp.float32) * inner_decay
        ).astype(jnp.bfloat16)
        within = jnp.dot(mixed, key_block, preferred_element_type=jnp.float32)
        across = (
            jnp.dot(grad_block, carried.astype(jnp.bfloat16).T, preferred_element_type=jnp.float32)
            * query_decay[:, None]
        )
        weighted = (key_block.astype(jnp.float32) * key_decay[:, None]).astype(jnp.bfloat16)
        updated = carried * block_decay + jnp.dot(
            weighted.T, value_block, preferred_element_type=jnp.float32
        )
        return (updated, (within + across, mixed))

    def backward(carried, inputs):
        query_block, key_block, value_block, grad_block, mixed = inputs
        scores = (
            jnp.dot(query_block, key_block.T, preferred_element_type=jnp.float32) * inner_decay
        ).astype(jnp.bfloat16)
        state_bf = carried.astype(jnp.bfloat16)
        grad_v = (
            jnp.dot(scores.T, grad_block, preferred_element_type=jnp.float32)
            + jnp.dot(key_block, state_bf, preferred_element_type=jnp.float32) * key_decay[:, None]
        )
        grad_k = (
            jnp.dot(mixed.T, query_block, preferred_element_type=jnp.float32)
            + jnp.dot(value_block, state_bf.T, preferred_element_type=jnp.float32)
            * key_decay[:, None]
        ) * scale
        weighted = (query_block.astype(jnp.float32) * query_decay[:, None]).astype(jnp.bfloat16)
        updated = carried * block_decay + jnp.dot(
            weighted.T, grad_block, preferred_element_type=jnp.float32
        )
        return (updated, (grad_k, grad_v))

    inputs = (
        split_blocks(queries),
        split_blocks(keys_scaled),
        split_blocks(values),
        split_blocks(cotangent),
    )
    initial = jnp.zeros((head_dim, values.shape[-1]), jnp.float32)
    final_state, (grad_q, mixed_all) = lax.scan(forward, initial, inputs)
    final_back, (grad_k, grad_v) = lax.scan(backward, initial, inputs + (mixed_all,), reverse=True)
    return (grad_q.reshape(length, -1), grad_k.reshape(length, -1), grad_v.reshape(length, -1))


def group_grads(log_rates, queries, key_rows, values, cotangent):
    length = queries.shape[0]
    head_count = log_rates.shape[0]

    def by_head(series):
        return series.reshape(length, head_count, -1).transpose(1, 0, 2)

    def to_rows(series):
        return series.transpose(1, 0, 2).reshape(length, -1)

    grad_q, grad_k, grad_v = jax.vmap(head_grads)(
        by_head(queries), by_head(key_rows), by_head(values), by_head(cotangent), log_rates
    )
    return jnp.concatenate((to_rows(grad_q), to_rows(grad_k), to_rows(grad_v)), axis=1).astype(
        jnp.bfloat16
    )


def body(hidden_in, mix_cotangent, query_weight, key_weight, value_weight, decay_log):
    own_rows = hidden_in[0]
    columns = query_weight.shape[1]
    stacked = jnp.stack((query_weight, key_weight, value_weight), axis=1)
    gathered = lax.all_gather(stacked, "dp", axis=0, tiled=True)
    weights = gathered.reshape(gathered.shape[0], 3 * columns)
    cotangent = lax.all_to_all(mix_cotangent[0], "sp", split_axis=1, concat_axis=0, tiled=True)
    all_rows = lax.all_gather(own_rows, "sp", axis=0, tiled=True)
    projected = jnp.dot(all_rows, weights, preferred_element_type=jnp.float32).astype(jnp.bfloat16)
    gradients = group_grads(
        decay_log,
        projected[:, :columns],
        projected[:, columns : 2 * columns],
        projected[:, 2 * columns :],
        cotangent,
    )
    input_sum = lax.psum_scatter(
        lax.dot_general(
            gradients, weights, (((1,), (1,)), ((), ())), preferred_element_type=jnp.float32
        ).astype(jnp.bfloat16),
        "sp",
        scatter_dimension=0,
        tiled=True,
    )
    grad_hidden = input_sum[None]
    summed = sent_and_summed(
        lax.dot_general(
            all_rows, gradients, (((0,), (0,)), ((), ())), preferred_element_type=jnp.float32
        ).astype(jnp.bfloat16),
        "dp",
        0,
    ) / lax.axis_size("dp")
    return (
        grad_hidden,
        summed[:, :columns],
        summed[:, columns : 2 * columns],
        summed[:, 2 * columns :],
    )


def solution(mesh):
    placed = (
        P("dp", "sp", None),
        P("dp", "sp", None),
        P("dp", "sp"),
        P("dp", "sp"),
        P("dp", "sp"),
        P("sp"),
    )
    return jax.shard_map(
        body,
        mesh=mesh,
        in_specs=placed,
        out_specs=(P("dp", "sp", None), P("dp", "sp"), P("dp", "sp"), P("dp", "sp")),
        check_vma=False,
    )
```

profile of v0, /device:TPU:1, one launch (start us, length us, event | category | flops | bytes accessed | tf_op | source)
XLA Modules:
  0.0 429.2 jit_solution(11572848178626721793)
XLA Ops:
  13.3 8.4 %all-to-all-start = ((bf16[128,16,256]{0,2,1:T(8,128)(2,1)}), bf16[128,16,256]{0,2,1:T(8,128)(2,1)S(1)}, u32[]{:S(2)}, u32[]{:S(2)}) async-start(bf16[128,16,256]{0,2,1:T(8,128)(2,1)} %bitcast.6), calls=%async_computation | async-start | bytes 2097152 | tf_op jit(solution)/shard_map/all_to_all | solution.py:110
  22.5 15.3 %all-to-all-done = bf16[128,16,256]{0,2,1:T(8,128)(2,1)S(1)} async-done(((bf16[128,16,256]{0,2,1:T(8,128)(2,1)}), bf16[128,16,256]{0,2,1:T(8,128)(2,1)S(1)}, u32[]{:S(2)}, u32[]{:S(2)}) %all-to-all-start) | async-done | bytes 1048608 | tf_op jit(solution)/shard_map/all_to_all | solution.py:110
  39.1 6.9 %all-gather.4.cloned.1.call-done = bf16[2048,3,256]{0,2,1:T(8,128)(2,1)} async-done(((bf16[256,3,256]{0,2,1:T(8,128)(2,1)}), bf16[2048,3,256]{0,2,1:T(8,128)(2,1)}) %all-gather.4.cloned.1.call-update) | async-done | bytes 3145744 | tf_op jit(solution)/shard_map/all_gather | solution.py:108
  46.0 73.5 %all-gather.6.cloned.1.call-done = bf16[1,2048,2048]{2,1,0:T(8,128)(2,1)} async-done(((bf16[1,128,2048]{2,1,0:T(8,128)(2,1)}), bf16[1,2048,2048]{2,1,0:T(8,128)(2,1)}) %all-gather.6.cloned.1.call-update) | async-done | bytes 8388624 | tf_op jit(solution)/shard_map/all_gather | solution.py:111
  119.5 10.1 %fusion.112 = bf16[2048,768]{0,1:T(8,128)(2,1)S(1)} fusion(bf16[2048,768]{0,1:T(8,128)(2,1)} %bitcast.220, bf16[1,2048,2048]{2,1,0:T(8,128)(2,1)} %all-gather.6.cloned.1.call-done), kind=kOutput, calls=%fused_computation.113 | convolution fusion | flops 6444023808 | bytes 14680064 | tf_op jit(solution)/shard_map/dot_general | solution.py:112
  133.9 95.3 %while.38 = (s32[]{:T(128)}, f32[1,256,256]{2,1,0:T(8,128)S(1)}, bf16[16,1,128,256]{3,2,1,0:T(8,128)(2,1)}, bf16[16,1,128,128]{3,2,1,0:T(8,128)(2,1)}, f32[1]{0:...) while((s32[]{:T(128)}, f32[1,256,256]{2,1,0:T(8,128)S(1)}, ...), condition=%wide.region_1.2_spmd.clone.clone.clone, body=%wide.region_0.1_spmd.clone.clone.clone.sunk | while | flops 50872832 | bytes 1677952 | solution.py:81
  133.9 2.4 bitcast_dynamic-update-slice_fusion.2
  139.9 2.3 bitcast_dynamic-update-slice_fusion.2
  145.9 2.3 bitcast_dynamic-update-slice_fusion.2
  151.8 2.3 bitcast_dynamic-update-slice_fusion.2
  157.8 2.3 bitcast_dynamic-update-slice_fusion.2
  163.7 2.3 bitcast_dynamic-update-slice_fusion.2
  169.7 2.3 bitcast_dynamic-update-slice_fusion.2
  175.6 2.3 bitcast_dynamic-update-slice_fusion.2
  181.6 2.3 bitcast_dynamic-update-slice_fusion.2
  187.5 2.3 bitcast_dynamic-update-slice_fusion.2
  193.5 2.3 bitcast_dynamic-update-slice_fusion.2
  199.4 2.3 bitcast_dynamic-update-slice_fusion.2
  205.4 2.3 bitcast_dynamic-update-slice_fusion.2
  211.3 2.3 bitcast_dynamic-update-slice_fusion.2
  217.3 2.3 bitcast_dynamic-update-slice_fusion.2
  223.2 2.3 bitcast_dynamic-update-slice_fusion.2
  230.7 96.6 %while.39 = (s32[]{:T(128)}, f32[1,256,256]{2,1,0:T(8,128)S(1)}, bf16[16,1,128,256]{3,2,1,0:T(8,128)(2,1)S(1)}, bf16[16,1,128,256]{3,2,1,0:T(8,128)(2,1)S(1)}, f...) while((s32[]{:T(128)}, f32[1,256,256]{2,1,0:T(8,128)S(1)}, ...), condition=%wide.region_3.4_spmd.clone.clone.clone, body=%wide.region_2.3_spmd.clone.clone.clone.sunk | while | flops 76202496 | bytes 2402974 | solution.py:82
  236.8 1.9 fusion.170
  254.9 1.9 fusion.170
  273.0 1.9 fusion.170
  291.1 1.9 fusion.170
  309.2 1.9 fusion.170
  327.3 10.9 %convolution_convert_fusion = bf16[2048,2048]{1,0:T(8,128)(2,1)} fusion(bf16[2048,768]{0,1:T(8,128)(2,1)} %bitcast.221, bf16[2048,256]{1,0:T(8,128)(2,1)S(1)} %bitcast.213, bf16[2048,256]{1,0:T(8,128)(2,1)S(1)} %bitcast.211, bf16[2048,256]{1,0:T(8,128)(2,1)} %bitcast.215), kind=kOutput, calls=%fused_computation.107 | convolution fusion | flops 6456082432 | bytes 14680064 | tf_op jit(solution)/shard_map/dot_general | solution.py:121
  339.4 9.1 %fusion.106 = bf16[768,2048]{1,0:T(8,128)(2,1)S(1)} fusion(bf16[1,2048,2048]{2,1,0:T(8,128)(2,1)} %all-gather.6.cloned.1.call-done, bf16[2048,256]{1,0:T(8,128)(2,1)S(1)} %bitcast.214, bf16[2048,256]{1,0:T(8,128)(2,1)S(1)} %bitcast.212, bf16[2048,256]{1,0:T(8,128)(2,1)S(1)} %bitcast.216), kind=kOutput, calls=%fused_computation.109 | convolution fusion | flops 6453460992 | bytes 14680064 | tf_op jit(solution)/shard_map/dot_general | solution.py:130
  348.7 42.3 %all_to_all.21 = bf16[8,256,768]{1,2,0:T(8,128)(2,1)S(1)} all-to-all(bf16[8,256,768]{1,2,0:T(8,128)(2,1)S(1)} %bitcast.205), channel_id=1, replica_groups=mesh['sp'=16,'dp'=8] {'dp'}, dimensions={0} | all-to-all | bytes 6291456 | tf_op jit(solution)/shard_map/all_to_all | solution.py:17
  394.1 28.5 %reduce-scatter.2.cloned.1.call-done = bf16[128,2048]{1,0:T(8,128)(2,1)} async-done(((bf16[2048,2048]{1,0:T(8,128)(2,1)}), bf16[128,2048]{1,0:T(8,128)(2,1)}) %reduce-scatter.2.cloned.1.call-update) | async-done | bytes 524304 | tf_op jit(solution)/shard_map/reduce_scatter | solution.py:120
  (191 shorter events, 161.7 us)
Async XLA Ops:
  7.2 4.7 %copy-start.1 = (bf16[1,128,4096]{2,1,0:T(8,128)(2,1)S(1)}, bf16[1,128,4096]{2,1,0:T(8,128)(2,1)}, u32[]{:S(2)}) copy-start(bf16[1,128,4096]{2,1,0:T(8,128)(2,1)} %param.11) | copy-start | bytes 3145732
  7.2 38.9 %all-gather.4.cloned.1.call-start = ((), (), s32[]{:S(2)}) async-start(), calls=%async_computation.3 | async-start | bytes 3538944 | tf_op jit(solution)/shard_map/all_gather | solution.py:108
  11.2 108.3 %all-gather.6.cloned.1.call-start = ((), (), s32[]{:S(2)}) async-start(), calls=%async_computation.5 | async-start | bytes 8912896 | tf_op jit(solution)/shard_map/all_gather | solution.py:111
  13.3 24.5 %all-to-all-start = ((bf16[128,16,256]{0,2,1:T(8,128)(2,1)}), bf16[128,16,256]{0,2,1:T(8,128)(2,1)S(1)}, u32[]{:S(2)}, u32[]{:S(2)}) async-start(bf16[128,16,256]{0,2,1:T(8,128)(2,1)} %bitcast.6), calls=%async_computation | async-start | bytes 2097152 | tf_op jit(solution)/shard_map/all_to_all | solution.py:110
  21.7 401.0 %reduce-scatter.2.cloned.1.call-start = ((), (), s32[]{:S(2)}) async-start(), calls=%async_computation.4 | async-start | bytes 8912896 | tf_op jit(solution)/shard_map/reduce_scatter | solution.py:120
  133.9 95.3 %copy-start = (bf16[2048,256]{0,1:T(8,128)(2,1)S(1)}, bf16[2048,256]{0,1:T(8,128)(2,1)}, u32[]{:S(2)}) copy-start(bf16[2048,256]{0,1:T(8,128)(2,1)} %get-tuple-element.631) | copy-start | bytes 3145732
  338.1 1.2 copy-start.2
Sparse Core Ops, SparseCore 0:
  11.3 34.7 all-gather.3
  48.2 71.2 all-gather.5
  338.3 84.3 reduce-scatter.1
where the time goes:
time: 436 us; the launch traced here: 429 us
  matrix products  199 us (46%)
  waiting for transfers between devices  125 us (29%)
  blocking collectives  42.3 us (10%)
  other arithmetic  22.6 us (5%)
  local copies, waits for them, and re-layouts  15.4 us (4%)
  between operations  14.6 us (3%)
  starting transfers between devices  8.54 us (2%)
    all_gather x1, waiting for transfers between devices, body(): all_rows = lax.all_gather(own_rows, 'sp', axis=0, tiled=True)  73.5 us
    all_to_all x1, blocking collectives, sent_and_summed(): lax.all_to_all(pieces, axis, split_axis=0, concat_axis=0, tiled=True)  42.3 us
    dot_general x16, matrix products, forward(): jnp.dot(grad_block, value_block.T, preferred_element_type=jnp.float32)  37.1 us
    dot_general x16, matrix products, backward(): jnp.dot(scores.T, grad_block, preferred_element_type=jnp.float32)  30.2 us
    reduce_scatter x1, waiting for transfers between devices, body(): lax.psum_scatter(lax.dot_general(gradients, weights, (((1,), (1,)), ((),...  28.5 us
    dot_general x16, matrix products, forward(): jnp.dot(grad_block, carried.astype(jnp.bfloat16).T, preferred_element_typ...  26.8 us
    dot_general x16, matrix products, backward(): jnp.dot(weighted.T, grad_block, preferred_element_type=jnp.float32)  18.6 us
    dot_general x16, matrix products, forward(): jnp.dot(weighted.T, value_block, preferred_element_type=jnp.float32)  18 us
  transfers between devices with their start and end apart: 4, of which 4 were waited for; matrix products, arithmetic and copies ran while one was open for 4% of the time, Pallas kernels for 0%

commit v1 on v0

v1 whole, which is shorter than its diff:
```python
import jax
import jax.numpy as jnp
from jax import lax
from jax.experimental import pallas as pl
from jax.experimental.pallas import tpu as pltpu
from jax.sharding import PartitionSpec as P

BLOCK = 128


def in_blocks(array, dim, size):
    shape = array.shape
    pieces = array.reshape(*shape[:dim], size, shape[dim] // size, *shape[dim + 1 :])
    return jnp.moveaxis(pieces, dim, 0)


def sent_and_summed(array, axis, dim):
    pieces = in_blocks(array, dim, lax.axis_size(axis))
    arrived = lax.all_to_all(pieces, axis, split_axis=0, concat_axis=0, tiled=True)
    return arrived.astype(jnp.float32).sum(axis=0)


def dot(a, b, dims):
    return lax.dot_general(a, b, ((dims[:1], dims[1:]), ((), ())), preferred_element_type=jnp.float32)


def retention_kernel(rate_ref, qkv_ref, cot_ref, out_ref, inner, qdec, kdec, fstate, bstate):
    length = qkv_ref.shape[0]
    hd = cot_ref.shape[1]
    blocks = length // BLOCK
    scale = hd ** (-0.5)
    rate = rate_ref[0]
    row = lax.broadcasted_iota(jnp.int32, (BLOCK, BLOCK), 0).astype(jnp.float32)
    col = lax.broadcasted_iota(jnp.int32, (BLOCK, BLOCK), 1).astype(jnp.float32)
    spread = row - col
    inner[...] = jnp.where(spread >= 0, jnp.exp(rate * jnp.maximum(spread, 0.0)), 0.0)
    rows = lax.broadcasted_iota(jnp.int32, (BLOCK, hd), 0).astype(jnp.float32)
    qdec[...] = jnp.exp(rate * (rows + 1.0))
    kdec[...] = jnp.exp(rate * (BLOCK - 1.0 - rows))
    step_decay = jnp.exp(jnp.full((hd, hd), rate * BLOCK, jnp.float32))
    fstate[...] = jnp.zeros_like(fstate)
    bstate[...] = jnp.zeros_like(bstate)

    def load(n):
        at = pl.ds(pl.multiple_of(n * BLOCK, BLOCK), BLOCK)
        q = qkv_ref[at, 0:hd]
        k = (qkv_ref[at, hd : 2 * hd].astype(jnp.float32) * scale).astype(jnp.bfloat16)
        v = qkv_ref[at, 2 * hd : 3 * hd]
        c = cot_ref[at, :]
        return at, q, k, v, c

    def step(i, _):
        at, q, k, v, c = load(i)
        mixed = (dot(c, v, (1, 1)) * inner[...]).astype(jnp.bfloat16)
        s = fstate[...]
        gq = dot(mixed, k, (1, 0)) + dot(c, s.astype(jnp.bfloat16), (1, 0)) * qdec[...]
        out_ref[at, 0:hd] = gq.astype(jnp.bfloat16)
        kw = (k.astype(jnp.float32) * kdec[...]).astype(jnp.bfloat16)
        fstate[...] = s * step_decay + dot(v, kw, (0, 0))

        at, q, k, v, c = load(blocks - 1 - i)
        mixed = (dot(c, v, (1, 1)) * inner[...]).astype(jnp.bfloat16)
        scores = (dot(q, k, (1, 1)) * inner[...]).astype(jnp.bfloat16)
        r = bstate[...]
        rb = r.astype(jnp.bfloat16)
        gv = dot(scores, c, (0, 0)) + dot(k, rb, (1, 0)) * kdec[...]
        gk = (dot(mixed, q, (0, 0)) + dot(v, rb, (1, 1)) * kdec[...]) * scale
        out_ref[at, hd : 2 * hd] = gk.astype(jnp.bfloat16)
        out_ref[at, 2 * hd : 3 * hd] = gv.astype(jnp.bfloat16)
        qw = (q.astype(jnp.float32) * qdec[...]).astype(jnp.bfloat16)
        bstate[...] = r * step_decay + dot(qw, c, (0, 0))
        return 0

    lax.fori_loop(0, blocks, step, 0)


def retention(rate, qkv, cotangent):
    length, hd = cotangent.shape
    return pl.pallas_call(
        retention_kernel,
        out_shape=jax.ShapeDtypeStruct(qkv.shape, jnp.bfloat16),
        in_specs=[
            pl.BlockSpec(memory_space=pltpu.SMEM),
            pl.BlockSpec(memory_space=pltpu.VMEM),
            pl.BlockSpec(memory_space=pltpu.VMEM),
        ],
        out_specs=pl.BlockSpec(memory_space=pltpu.VMEM),
        scratch_shapes=[
            pltpu.VMEM((BLOCK, BLOCK), jnp.float32),
            pltpu.VMEM((BLOCK, hd), jnp.float32),
            pltpu.VMEM((BLOCK, hd), jnp.float32),
            pltpu.VMEM((hd, hd), jnp.float32),
            pltpu.VMEM((hd, hd), jnp.float32),
        ],
        cost_estimate=pl.CostEstimate(flops=2_000_000_000, bytes_accessed=8_000_000, transcendentals=0),
    )(rate, qkv, cotangent)


def body(hidden_in, mix_cotangent, query_weight, key_weight, value_weight, decay_log):
    own_rows = hidden_in[0]
    columns = query_weight.shape[1]
    stacked = jnp.stack((query_weight, key_weight, value_weight), axis=1)
    gathered = lax.all_gather(stacked, "dp", axis=0, tiled=True)
    weights = gathered.reshape(gathered.shape[0], 3 * columns)
    cotangent = lax.all_to_all(mix_cotangent[0], "sp", split_axis=1, concat_axis=0, tiled=True)
    all_rows = lax.all_gather(own_rows, "sp", axis=0, tiled=True)
    projected = jnp.dot(all_rows, weights, preferred_element_type=jnp.float32).astype(jnp.bfloat16)
    gradients = retention(decay_log, projected, cotangent)
    input_sum = lax.psum_scatter(
        lax.dot_general(
            gradients, weights, (((1,), (1,)), ((), ())), preferred_element_type=jnp.float32
        ).astype(jnp.bfloat16),
        "sp",
        scatter_dimension=0,
        tiled=True,
    )
    grad_hidden = input_sum[None]
    summed = sent_and_summed(
        lax.dot_general(
            all_rows, gradients, (((0,), (0,)), ((), ())), preferred_element_type=jnp.float32
        ).astype(jnp.bfloat16),
        "dp",
        0,
    ) / lax.axis_size("dp")
    return (
        grad_hidden,
        summed[:, :columns],
        summed[:, columns : 2 * columns],
        summed[:, 2 * columns :],
    )


def solution(mesh):
    placed = (
        P("dp", "sp", None),
        P("dp", "sp", None),
        P("dp", "sp"),
        P("dp", "sp"),
        P("dp", "sp"),
        P("sp"),
    )
    return jax.shard_map(
        body,
        mesh=mesh,
        in_specs=placed,
        out_specs=(P("dp", "sp", None), P("dp", "sp"), P("dp", "sp"), P("dp", "sp")),
        check_vma=False,
    )
```

time: 436 us -> 250 us (0.57); the launches traced: 429 us -> 249 us
  matrix products: 199 us -> 31.6 us
  other arithmetic: 22.6 us -> 1.29 us
  Pallas kernels: 0 us -> 14.5 us
  local copies, waits for them, and re-layouts: 15.4 us -> 10.3 us
    dot_general x144 -> x0, matrix products: 169 us -> none  [the longest x16 37.1 us: forward(): jnp.dot(grad_block, value_block.T, preferred_element_type=jnp.float32)]
    mul x32 -> x0, other arithmetic: 21.1 us -> none  [the longest x16 10.6 us: backward(): jnp.dot(value_block, state_bf.T, preferred_element_type=jnp.float32)]
    all_gather x1, waiting for transfers between devices: 6.94 us -> 23.4 us  [body(): gathered = lax.all_gather(stacked, 'dp', axis=0, tiled=True)]
    all_to_all x1, waiting for transfers between devices: 15.3 us -> 0.01 us  [body(): lax.all_to_all(mix_cotangent[0], 'sp', split_axis=1, concat_axis=0, tiled...]
    pallas_call x0 -> x1, Pallas kernels: none -> 14.5 us  [retention(): pl.pallas_call(retention_kernel, out_shape=jax.ShapeDtypeStruct(qkv.shape...]
    unnamed x17 -> x13, local copies, waits for them, and re-layouts: 12.7 us -> 8.72 us
  transfers between devices with their start and end apart: 4 -> 4, of which waited for: 4 -> 3; matrix products, arithmetic and copies ran while one was open for 4% -> 10% of each run, Pallas kernels for 0% -> 0%
where the time goes in v1:
time: 250 us; the launch traced here: 249 us
  waiting for transfers between devices  125 us (50%)
  blocking collectives  42.4 us (17%)
  matrix products  31.6 us (13%)
  Pallas kernels  14.5 us (6%)
  between operations  14.5 us (6%)
  local copies, waits for them, and re-layouts  10.3 us (4%)
  starting transfers between devices  8.54 us (3%)
    all_gather x1, waiting for transfers between devices, body(): all_rows = lax.all_gather(own_rows, 'sp', axis=0, tiled=True)  73.5 us
    all_to_all x1, blocking collectives, sent_and_summed(): lax.all_to_all(pieces, axis, split_axis=0, concat_axis=0, tiled=True)  42.4 us
    reduce_scatter x1, waiting for transfers between devices, body(): lax.psum_scatter(lax.dot_general(gradients, weights, (((1,), (1,)), ((),...  27.8 us
    all_gather x1, waiting for transfers between devices, body(): gathered = lax.all_gather(stacked, 'dp', axis=0, tiled=True)  23.4 us
    pallas_call x1, Pallas kernels, retention(): pl.pallas_call(retention_kernel, out_shape=jax.ShapeDtypeStruct(qkv.shape...  14.5 us
    dot_general x1, matrix products, body(): lax.dot_general(gradients, weights, (((1,), (1,)), ((), ())), preferred_e...  11.3 us
    dot_general x1, matrix products, body(): jnp.dot(all_rows, weights, preferred_element_type=jnp.float32)  11.2 us
    dot_general x1, matrix products, body(): lax.dot_general(all_rows, gradients, (((0,), (0,)), ((), ())), preferred_...  9.14 us
  transfers between devices with their start and end apart: 4, of which 3 were waited for; matrix products, arithmetic and copies ran while one was open for 10% of the time, Pallas kernels for 0%

profile of v1, /device:TPU:1, one launch (start us, length us, event | category | flops | bytes accessed | tf_op | source)
XLA Modules:
  0.0 248.5 jit_solution(12025215417735468505)
XLA Ops:
  7.2 0.0 all-gather.4.cloned.1.call-start
  7.2 1.1 copy.17
  8.3 1.0 copy.18
  9.3 1.0 copy.19
  10.3 0.8 pad_maximum_fusion
  11.1 0.0 all-gather.4.cloned.1.call-update
  11.1 0.0 all-gather.6.cloned.1.call-start
  11.2 0.7 all-gather.6.cloned.1.call-update
  11.9 0.0 copy-done
  11.9 0.2 copy.30
  12.2 1.3 copy.21
  13.5 8.4 %all-to-all-start = ((bf16[128,16,256]{2,0,1:T(8,128)(2,1)}), bf16[128,16,256]{2,0,1:T(8,128)(2,1)S(1)}, u32[]{:S(2)}, u32[]{:S(2)}) async-start(bf16[128,16,256]{2,0,1:T(8,128)(2,1)} %copy.21), calls=%async_computation | async-start | bytes 2097152 | tf_op jit(solution)/shard_map/all_to_all | solution.py:105
  21.9 0.0 reduce-scatter.2.cloned.1.call-start
  22.6 23.4 %all-gather.4.cloned.1.call-done = bf16[2048,3,256]{0,2,1:T(8,128)(2,1)} async-done(((bf16[256,3,256]{0,2,1:T(8,128)(2,1)}), bf16[2048,3,256]{0,2,1:T(8,128)(2,1)}) %all-gather.4.cloned.1.call-update) | async-done | bytes 3145744 | tf_op jit(solution)/shard_map/all_gather | solution.py:103
  46.0 73.5 %all-gather.6.cloned.1.call-done = bf16[1,2048,2048]{2,1,0:T(8,128)(2,1)} async-done(((bf16[1,128,2048]{2,1,0:T(8,128)(2,1)}), bf16[1,2048,2048]{2,1,0:T(8,128)(2,1)}) %all-gather.6.cloned.1.call-update) | async-done | bytes 8388624 | tf_op jit(solution)/shard_map/all_gather | solution.py:106
  119.5 11.2 %fusion.10.qkv_ref = bf16[2048,768]{1,0:T(8,128)(2,1)} fusion(bf16[2048,768]{0,1:T(8,128)(2,1)} %bitcast.41, bf16[1,2048,2048]{2,1,0:T(8,128)(2,1)} %all-gather.6.cloned.1.call-done), kind=kOutput, calls=%fused_computation.9 | convolution fusion | flops 6444023808 | bytes 14680064 | tf_op jit(solution)/shard_map/dot_general | solution.py:107
  130.7 0.0 all-to-all-done
  130.7 1.0 copy-done.1
  131.7 14.5 %shard_map.93 = bf16[2048,768]{1,0:T(8,128)(2,1)} custom-call(f32[1]{0:T(128)S(6)} %copy.33.rate_ref, bf16[2048,768]{1,0:T(8,128)(2,1)} %fusion.10.qkv_ref, bf16[2048,256]{1,0:T(8,128)(2,1)} %bitcast.37), custom_call_target="tpu_custom_call" | custom-call | flops 2000000000 | bytes 8000000 | tf_op jit(solution)/shard_map/pallas_call | solution.py:79
  146.2 11.3 %convolution_convert_fusion = bf16[2048,2048]{1,0:T(8,128)(2,1)} fusion(bf16[2048,768]{1,0:T(8,128)(2,1)} %shard_map.93, bf16[2048,768]{0,1:T(8,128)(2,1)} %bitcast.42), kind=kOutput, calls=%fused_computation.4 | convolution fusion | flops 6446645248 | bytes 14680064 | tf_op jit(solution)/shard_map/dot_general | solution.py:110
  157.4 0.0 reduce-scatter.2.cloned.1.call-update
  157.5 1.9 copy-done.2
  159.3 9.1 %fusion.7 = bf16[768,2048]{1,0:T(8,128)(2,1)S(1)} fusion(bf16[2048,768]{1,0:T(8,128)(2,1)S(1)} %copy-done.2, bf16[1,2048,2048]{2,1,0:T(8,128)(2,1)} %all-gather.6.cloned.1.call-done), kind=kOutput, calls=%fused_computation.7 | convolution fusion | flops 6444023808 | bytes 14680064 | tf_op jit(solution)/shard_map/dot_general | solution.py:119
  168.5 0.2 copy.32
  168.7 42.4 %all_to_all.24 = bf16[8,256,768]{1,2,0:T(8,128)(2,1)S(1)} all-to-all(bf16[8,256,768]{1,2,0:T(8,128)(2,1)S(1)} %bitcast.33), channel_id=1, replica_groups=mesh['sp'=16,'dp'=8] {'dp'}, dimensions={0} | all-to-all | bytes 6291456 | tf_op jit(solution)/shard_map/all_to_all | solution.py:19
  211.1 0.4 convert_reduce_fusion
  211.5 0.1 broadcast_multiply_fusion
  211.6 0.1 fusion.13
  211.6 0.8 copy.26
  212.5 0.8 copy.25
  213.3 0.8 copy.24
  214.2 27.8 %reduce-scatter.2.cloned.1.call-done = bf16[128,2048]{1,0:T(8,128)(2,1)} async-done(((bf16[2048,2048]{1,0:T(8,128)(2,1)}), bf16[128,2048]{1,0:T(8,128)(2,1)}) %reduce-scatter.2.cloned.1.call-update) | async-done | bytes 524304 | tf_op jit(solution)/shard_map/reduce_scatter | solution.py:109
  (3 shorter events, 0.0 us)
Async XLA Ops:
  7.2 4.7 %copy-start = (bf16[1,128,4096]{2,1,0:T(8,128)(2,1)S(1)}, bf16[1,128,4096]{2,1,0:T(8,128)(2,1)}, u32[]{:S(2)}) copy-start(bf16[1,128,4096]{2,1,0:T(8,128)(2,1)} %param.7) | copy-start | bytes 3145732
  7.2 38.9 %all-gather.4.cloned.1.call-start = ((), (), s32[]{:S(2)}) async-start(), calls=%async_computation.3 | async-start | bytes 3538944 | tf_op jit(solution)/shard_map/all_gather | solution.py:103
  11.1 108.3 %all-gather.6.cloned.1.call-start = ((), (), s32[]{:S(2)}) async-start(), calls=%async_computation.5 | async-start | bytes 8912896 | tf_op jit(solution)/shard_map/all_gather | solution.py:106
  13.5 117.2 %all-to-all-start = ((bf16[128,16,256]{2,0,1:T(8,128)(2,1)}), bf16[128,16,256]{2,0,1:T(8,128)(2,1)S(1)}, u32[]{:S(2)}, u32[]{:S(2)}) async-start(bf16[128,16,256]{2,0,1:T(8,128)(2,1)} %copy.21), calls=%async_computation | async-start | bytes 2097152 | tf_op jit(solution)/shard_map/all_to_all | solution.py:105
  21.9 220.0 %reduce-scatter.2.cloned.1.call-start = ((), (), s32[]{:S(2)}) async-start(), calls=%async_computation.4 | async-start | bytes 8912896 | tf_op jit(solution)/shard_map/reduce_scatter | solution.py:109
  130.7 1.0 copy-start.1
  157.4 1.9 copy-start.2
Sparse Core Ops, SparseCore 0:
  11.3 34.7 all-gather.3
  48.2 71.2 all-gather.5
  157.6 84.3 reduce-scatter.1

commit v2 on v1

v2 whole, which is shorter than its diff:
```python
import jax
import jax.numpy as jnp
from jax import lax
from jax.experimental import pallas as pl
from jax.experimental.pallas import tpu as pltpu
from jax.sharding import PartitionSpec as P

BLOCK = 128
COPIES = 96
BF16 = jnp.bfloat16
F32 = jnp.float32


def dot(a, b, dims):
    return lax.dot_general(a, b, ((dims[:1], dims[1:]), ((), ())), preferred_element_type=F32)


def both(a, b):
    return (a.astype(F32) + b.astype(F32)).astype(BF16)


def offset(q):
    return jnp.where(q == 0, 2, jnp.where(q == 1, 1, jnp.where(q == 2, 3, 0)))


def kernel(
    rate_ref, hid, cot, wq, wk, wv,
    dx_out, dq_out, dk_out, dv_out,
    X, W, C, QKV, G, GT, PX, RB, EZ, FU, FD, SU, SD, EX, FIN, RFIN,
    DW, YFU, YFD, YSU, YSD, HB0, HB1, RT, PR, inner, qdec, kdec, sdec, fstate, bstate,
    ss, rs, csend, crecv, lsem,
):
    hd = wq.shape[1]
    depth = wq.shape[0]
    s = lax.axis_index("sp")
    d = lax.axis_index("dp")
    z, x = s // 4, s % 4
    y, c = d // 2, d % 2
    g = x // 2
    r = (c + g) % 2
    xp = x + 1 - 2 * (x % 2)
    j = z * 2 + x % 2
    up, down, far = (z + 1) % 4, (z + 3) % 4, (z + 2) % 4
    yu, yd, yf = (y + 1) % 4, (y + 3) % 4, (y + 2) % 4

    def at(zz, xx):
        return zz * 2 + xx % 2

    def dev(sp, dp):
        return {"sp": sp, "dp": dp}

    pair = dev(z * 4 + xp, d)
    zup, zdown = dev(up * 4 + x, d), dev(down * 4 + x, d)
    yup, ydown = dev(s, yu * 2 + c), dev(s, yd * 2 + c)
    sibling = dev(s, y * 2 + 1 - c)
    swap = z * 4 + 3 - x
    copies = {}

    def add(name, src, dst, device, landing=None):
        n = len(copies)
        copies[name] = pltpu.make_async_remote_copy(
            src_ref=src, dst_ref=dst, send_sem=ss.at[n], recv_sem=rs.at[n if landing is None else landing],
            device_id=device, device_id_type=pl.DeviceIdType.MESH,
        )

    def start(*names):
        for name in names:
            copies[name].start()

    def arrived(*names):
        for name in names:
            copies[name].wait_recv()

    half = BLOCK // 2
    quarter = BLOCK // 4
    xr, zr = pl.ds(0, half), pl.ds(half, half)

    def blk(zz, xx, rows):
        return X.at[2 * at(zz, xx) + r, rows]

    def ring(name, device, src):
        add(name, src, src, device)

    add("swap_x", hid.at[0], X.at[2 * at(z, 3 - x) + 1], dev(swap, y * 2 + 1 - c))
    ring("A", pair, blk(z, x, xr))
    for tag, xx, rows, o in (("z", x, zr, half), ("a", x, xr, 0), ("b", xp, xr, 0)):
        ring(tag + "u", zup, blk(z, xx, rows))
        ring(tag + "d", zdown, blk(z, xx, rows))
        ring(tag + "uu", zup, blk(down, xx, pl.ds(o, quarter)))
        ring(tag + "dd", zdown, blk(up, xx, pl.ds(o + quarter, quarter)))
    for tag, zz in (("H0", z), ("H1", down), ("H2", up), ("H3", far)):
        ring(tag, pair, blk(zz, x, zr))
    order = [(z, x), (down, x), (up, x), (far, x), (z, xp), (down, xp), (up, xp), (far, xp)]
    for n, (zz, xx) in enumerate(order):
        slot = X.at[2 * at(zz, xx) + r]
        add("D%d" % n, slot, slot, sibling)

    for n, w in enumerate((wq, wk, wv)):
        cols = pl.ds(n * hd, hd)
        add("own_w%d" % n, w, W.at[d, :, cols], sibling)
        add("swap_w%d" % n, w, W.at[d, :, cols], dev(swap, y * 2 + g), COPIES + 2 * n + c)
    for i in range(2):
        ring("wu%d" % i, yup, W.at[2 * y + i])
        ring("wd%d" % i, ydown, W.at[2 * y + i])
    ring("wuu", yup, W.at[2 * yd])
    ring("wdd", ydown, W.at[2 * yu + 1])
    add("rate", RT, PR, dev(swap, d))

    def out(zz, xx, rows):
        return RB.at[at(zz, xx), rows]

    porder = [(far, xp), (far, x), (up, xp), (up, x), (down, xp), (down, x), (z, xp), (z, x)]
    for n, (zz, xx) in enumerate(porder):
        add("P%d" % n, PX.at[2 * at(zz, xx) + 1 - r], RB.at[at(zz, xx)], sibling)
    for n, zz in enumerate((far, up, down, z)):
        add("EZ%d" % n, out(zz, xp, zr), EZ.at[zz], pair)
    cols3 = ((0, x, 0), (1, xp, 0), (2, x, half))
    for m, xx, o in cols3:
        add("FU%d" % m, out(far, xx, pl.ds(o, quarter)), FU.at[m], zup)
        add("FD%d" % m, out(far, xx, pl.ds(o + quarter, quarter)), FD.at[m], zdown)
        add("SU%d" % m, out(up, xx, pl.ds(o, half)), SU.at[m], zup)
        add("SD%d" % m, out(down, xx, pl.ds(o, half)), SD.at[m], zdown)
    add("EX", out(z, xp, xr), EX, pair)
    for n, rows in enumerate((xr, zr)):
        add("fin%d" % n, FIN.at[rows], RFIN.at[rows], dev(swap, y * 2 + 1 - c))

    add("YFU", DW.at[2 * yf], YFU, yup)
    add("YFD", DW.at[2 * yf + 1], YFD, ydown)
    for i in range(2):
        add("YSU%d" % i, DW.at[2 * yu + i], YSU.at[i], yup)
        add("YSD%d" % i, DW.at[2 * yd + i], YSD.at[i], ydown)
        add("hb1_%d" % i, DW.at[2 * y + i], HB1, dev(swap, 2 * y + i), COPIES + 6)
    add("hb0", DW.at[2 * y + 1 - c], HB0, sibling)

    RT[...] = jnp.full(RT.shape, rate_ref[0], F32)

    own_x = X.at[2 * j + r]
    local_x = pltpu.make_async_copy(hid.at[0], X.at[2 * j], rs.at[0])

    @pl.when(r == 0)
    def _():
        local_x.start()

    @pl.when(r == 1)
    def _():
        start("swap_x")

    for n, w in enumerate((wq, wk, wv)):
        start("swap_w%d" % n)

    @pl.when(r == 0)
    def _():
        for n, w in enumerate((wq, wk, wv)):
            pltpu.make_async_copy(w, W.at[d, :, pl.ds(n * hd, hd)], lsem.at[n]).start()

    @pl.when(r == 1)
    def _():
        for n in range(3):
            start("own_w%d" % n)

    pltpu.make_async_copy(own_x, own_x, rs.at[0]).wait()
    start("A", "zu", "zd", "H0", "au", "ad", "D0")

    bx = x + r * (3 - 2 * x)
    cslot = 2 * (z * 2 + bx - 2 * c) + r

    def cot_copy(k):
        h = (s + k) % 16
        hz, hx = h // 4, h % 4
        role = (hx // 2 + c) % 2
        tx = hx + role * (3 - 2 * hx)
        tc = c + role * (1 - 2 * c)
        src = cot.at[0, :, pl.ds(pl.multiple_of(h * hd, hd), hd)]
        same = jnp.logical_and(r == 0, k == 0)
        return same, src, dev(hz * 4 + tx, 2 * y + tc), csend.at[k]

    def cot_send(k, _):
        same, src, device, sem = cot_copy(k)

        @pl.when(same)
        def _():
            pltpu.make_async_copy(src, C.at[cslot], crecv).start()

        @pl.when(jnp.logical_not(same))
        def _():
            pltpu.make_async_remote_copy(
                src_ref=src, dst_ref=C.at[cslot], send_sem=sem, recv_sem=crecv,
                device_id=device, device_id_type=pl.DeviceIdType.MESH,
            ).start()

        return 0

    lax.fori_loop(0, 16, cot_send, 0)
    start("rate")

    arrived("A")
    start("bu", "bd")

    @pl.when(r == 0)
    def _():
        for n, w in enumerate((wq, wk, wv)):
            pltpu.make_async_copy(w, W.at[d, :, pl.ds(n * hd, hd)], lsem.at[n]).wait()
        arrived("own_w0", "own_w1", "own_w2")

    @pl.when(r == 1)
    def _():
        for n in range(3):
            for i in range(2):
                piece = W.at[2 * y + i, :, pl.ds(n * hd, hd)]
                pltpu.make_async_copy(piece, piece, rs.at[COPIES + 2 * n + i]).wait()

    start("wu0", "wd1", "wu1", "wd0")

    arrived("zu")
    start("zuu", "H1")
    arrived("zd")
    start("zdd", "H2")
    arrived("au")
    start("auu", "D1")
    arrived("ad")
    start("add", "D2")
    arrived("bu")
    start("buu")
    arrived("bd")
    start("bdd")
    arrived("zuu", "zdd")
    start("H3")
    arrived("wu0")
    start("wuu")
    arrived("wd1")
    start("wdd")
    arrived("auu", "add")
    start("D3")
    arrived("H0")
    start("D4")
    arrived("wu1", "wd0", "wuu", "wdd")

    def project(k, _):
        @pl.when(k == 3)
        def _():
            arrived("H1")
            start("D5")
            arrived("H2")
            start("D6")

        @pl.when(k == 6)
        def _():
            arrived("buu", "bdd", "H3")
            start("D7")

        for n in range(8):

            @pl.when(k == n)
            def _():
                arrived("D%d" % n)

        q = k % 4
        zz = (z + jnp.where(q == 0, 0, jnp.where(q == 1, 3, jnp.where(q == 2, 1, 2)))) % 4
        jj = at(zz, x + k // 4)
        rows = pl.ds(2 * jj, 2)
        a = X[rows].reshape(2 * BLOCK, X.shape[2])
        for n in range(3):
            b = W[:, :, n * hd : (n + 1) * hd].reshape(X.shape[2], hd)
            QKV[rows, :, n * hd : (n + 1) * hd] = dot(a, b, (1, 0)).astype(BF16).reshape(2, BLOCK, hd)
        return 0

    lax.fori_loop(0, 8, project, 0)

    arrived("rate")
    pltpu.make_async_copy(C, C, crecv).wait()
    rate = jnp.where(r == 0, RT[0:1, :], PR[0:1, :])
    row = lax.broadcasted_iota(jnp.int32, (BLOCK, BLOCK), 0).astype(F32)
    col = lax.broadcasted_iota(jnp.int32, (BLOCK, BLOCK), 1).astype(F32)
    spread = row - col
    inner[...] = jnp.where(spread >= 0, jnp.exp(rate * jnp.maximum(spread, 0.0)), 0.0)
    qd = jnp.exp(rate * (row + 1.0))
    kd = jnp.exp(rate * (BLOCK - 1.0 - row))
    qdec[...] = jnp.concatenate((qd, qd), axis=1)
    kdec[...] = jnp.concatenate((kd, kd), axis=1)
    sd = jnp.exp(rate * float(BLOCK))
    sdec[...] = jnp.concatenate((sd, sd), axis=1)
    fstate[...] = jnp.zeros_like(fstate)
    bstate[...] = jnp.zeros_like(bstate)
    scale = hd ** (-0.5)
    blocks = X.shape[0]

    def load(n):
        px = n % 4
        role = (px // 2 + g) % 2
        slot = 2 * at(n // 4, px + role * (3 - 2 * px)) + role
        q = QKV[slot, :, 0:hd]
        k = (QKV[slot, :, hd : 2 * hd].astype(F32) * scale).astype(BF16)
        v = QKV[slot, :, 2 * hd : 3 * hd]
        return slot, q, k, v, C[slot]

    def put(slot, n, value):
        value = value.astype(BF16)
        G[slot, :, n * hd : (n + 1) * hd] = value
        lanes = pl.ds(pl.multiple_of(slot * BLOCK, BLOCK), BLOCK)
        GT[n * hd : (n + 1) * hd, lanes] = value.T

    def retain(i, _):
        slot, q, k, v, ct = load(i)
        mixed = (dot(ct, v, (1, 1)) * inner[...]).astype(BF16)
        st = fstate[...]
        put(slot, 0, dot(mixed, k, (1, 0)) + dot(ct, st.astype(BF16), (1, 0)) * qdec[...])
        kw = (k.astype(F32) * kdec[...]).astype(BF16)
        fstate[...] = st * sdec[...] + dot(v, kw, (0, 0))

        slot, q, k, v, ct = load(blocks - 1 - i)
        mixed = (dot(ct, v, (1, 1)) * inner[...]).astype(BF16)
        scores = (dot(q, k, (1, 1)) * inner[...]).astype(BF16)
        st = bstate[...]
        sb = st.astype(BF16)
        put(slot, 1, (dot(mixed, q, (0, 0)) + dot(v, sb, (1, 1)) * kdec[...]) * scale)
        put(slot, 2, dot(scores, ct, (0, 0)) + dot(k, sb, (1, 0)) * kdec[...])
        qw = (q.astype(F32) * qdec[...]).astype(BF16)
        bstate[...] = st * sdec[...] + dot(qw, ct, (0, 0))
        return 0

    lax.fori_loop(0, blocks, retain, 0)

    def chip_sum(n):
        zz, xx = porder[n]
        arrived("P%d" % n)
        jj = at(zz, xx)
        RB[jj] = both(RB[jj], PX[2 * jj + r])

    def merge(ref, index, rows, other):
        ref[index, rows] = both(ref[index, rows], other)

    def ring_up(m):
        _, xx, o = cols3[m]
        arrived("FU%d" % m)
        merge(RB, at(up, xx), pl.ds(o, quarter), FU[m])
        start("SU%d" % m)

    def ring_down(m):
        _, xx, o = cols3[m]
        arrived("FD%d" % m)
        merge(RB, at(down, xx), pl.ds(o + quarter, quarter), FD[m])
        start("SD%d" % m)

    def pair_in(n):
        zz = (far, up, down, z)[n]
        arrived("EZ%d" % n)
        merge(RB, at(zz, x), zr, EZ[zz])

    def yblock(k):
        yo = jnp.where(k < 2, 2, jnp.where(k < 6, jnp.where(k % 2 == 0, 1, 3), 0))
        i = jnp.where(jnp.logical_or(k == 2, k == 3), (k + 1) % 2, k % 2)
        return 2 * ((y + yo) % 4) + i

    def products(k, _):
        jj = at((z + offset(k // 2)) % 4, x + 1 - k % 2)
        rows = pl.ds(2 * jj, 2)
        a = G[rows].reshape(2 * BLOCK, 3 * hd)
        for n in range(8):
            piece = dot(a, W[n], (1, 1)).astype(BF16)
            PX[rows, :, n * depth : (n + 1) * depth] = piece.reshape(2, BLOCK, depth)
        for n in range(8):

            @pl.when(k == n)
            def _():
                start("P%d" % n)

        db = yblock(k)
        cols = pl.ds(pl.multiple_of(db * depth, depth), depth)
        b = X[:, :, cols].reshape(blocks * BLOCK, depth)
        for n in range(3):
            part = pl.ds(n * hd, hd)
            DW[db, part, :] = dot(GT[part, :], b, (1, 0)).astype(BF16)

        @pl.when(k == 0)
        def _():
            start("YFU")
            chip_sum(0)
            start("EZ0", "FU1", "FD1")

        @pl.when(k == 1)
        def _():
            start("YFD")
            chip_sum(1)
            start("FU0", "FD0")

        @pl.when(k == 2)
        def _():
            start("YSU1")
            chip_sum(2)
            start("EZ1")

        @pl.when(k == 3)
        def _():
            start("YSD0")
            chip_sum(3)
            ring_up(1)

        @pl.when(k == 4)
        def _():
            chip_sum(4)
            start("EZ2")
            ring_down(1)
            ring_up(0)

        @pl.when(k == 5)
        def _():
            chip_sum(5)
            ring_down(0)
            pair_in(0)
            start("FU2", "FD2")
            arrived("YFU")
            DW[2 * yu] = both(DW[2 * yu], YFU[...])
            start("YSU0")

        @pl.when(k == 6)
        def _():
            arrived("YFD")
            DW[2 * yd + 1] = both(DW[2 * yd + 1], YFD[...])
            start("YSD1")
            chip_sum(6)
            start("EZ3")
            pair_in(1)
            ring_up(2)

        @pl.when(k == 7)
        def _():
            chip_sum(7)
            pair_in(2)
            ring_down(2)

        return 0

    lax.fori_loop(0, 8, products, 0)

    arrived("SU1", "SD1")
    jp = at(z, xp)
    RB[jp, xr] = (RB[jp, xr].astype(F32) + SU[1].astype(F32) + SD[1].astype(F32)).astype(BF16)
    start("EX")
    arrived("SU0", "SD0", "EX")
    total = RB[j, xr].astype(F32) + SU[0].astype(F32) + SD[0].astype(F32) + EX[...].astype(F32)
    FIN[xr] = total.astype(BF16)

    @pl.when(r == 1)
    def _():
        start("fin0")

    arrived("YSU1", "YSD0", "YSU0", "YSD1")
    for i in range(2):
        total = DW[2 * y + i].astype(F32) + YSU[i].astype(F32) + YSD[i].astype(F32)
        DW[2 * y + i] = total.astype(BF16)

    @pl.when(r == 0)
    def _():
        start("hb0")

    @pl.when(r == 1)
    def _():
        start("hb1_0", "hb1_1")

    pair_in(3)
    arrived("SU2", "SD2")
    total = RB[j, zr].astype(F32) + SU[2].astype(F32) + SD[2].astype(F32)
    FIN[zr] = total.astype(BF16)

    @pl.when(r == 0)
    def _():
        dx_out[0] = FIN[...]

    @pl.when(r == 1)
    def _():
        start("fin1")

    copies["hb1_0"].wait_recv()

    def weights_out(part):
        for n, ref in enumerate((dq_out, dk_out, dv_out)):
            rows = pl.ds(n * hd, hd)
            ref[...] = ((part[rows].astype(F32) + HB1[rows].astype(F32)) * 0.125).T

    @pl.when(r == 0)
    def _():
        weights_out(DW.at[2 * y + c])

    @pl.when(r == 1)
    def _():
        arrived("hb0")
        weights_out(HB0)
        arrived("fin0", "fin1")
        dx_out[0] = RFIN[...]

    only_one = ("swap_x", "own_w0", "own_w1", "own_w2", "fin0", "fin1", "hb1_0", "hb1_1")
    for name in copies:
        if name not in only_one and name != "hb0":
            copies[name].wait_send()

    @pl.when(r == 1)
    def _():
        for name in only_one:
            copies[name].wait_send()

    @pl.when(r == 0)
    def _():
        copies["hb0"].wait_send()

    def cot_done(k, _):
        same, src, device, sem = cot_copy(k)

        @pl.when(jnp.logical_not(same))
        def _():
            pltpu.make_async_remote_copy(
                src_ref=src, dst_ref=C.at[cslot], send_sem=sem, recv_sem=crecv,
                device_id=device, device_id_type=pl.DeviceIdType.MESH,
            ).wait_send()

        return 0

    lax.fori_loop(0, 16, cot_done, 0)


def body(hidden_in, mix_cotangent, query_weight, key_weight, value_weight, decay_log):
    model = hidden_in.shape[2]
    depth, hd = query_weight.shape
    ways = model // depth
    slots = 16
    vmem = pltpu.VMEM
    any_space = pl.BlockSpec(memory_space=pl.ANY)
    whole = pl.BlockSpec(memory_space=pltpu.VMEM)
    grad = jax.ShapeDtypeStruct((depth, hd), F32)
    return pl.pallas_call(
        kernel,
        out_shape=(jax.ShapeDtypeStruct(hidden_in.shape, BF16), grad, grad, grad),
        in_specs=[pl.BlockSpec(memory_space=pltpu.SMEM)] + [any_space] * 5,
        out_specs=(whole,) * 4,
        scratch_shapes=[
            vmem((slots, BLOCK, model), BF16),
            vmem((ways, depth, 3 * hd), BF16),
            vmem((slots, BLOCK, hd), BF16),
            vmem((slots, BLOCK, 3 * hd), BF16),
            vmem((slots, BLOCK, 3 * hd), BF16),
            vmem((3 * hd, slots * BLOCK), BF16),
            vmem((slots, BLOCK, model), BF16),
            vmem((slots // 2, BLOCK, model), BF16),
            vmem((4, BLOCK // 2, model), BF16),
            vmem((3, BLOCK // 4, model), BF16),
            vmem((3, BLOCK // 4, model), BF16),
            vmem((3, BLOCK // 2, model), BF16),
            vmem((3, BLOCK // 2, model), BF16),
            vmem((BLOCK // 2, model), BF16),
            vmem((BLOCK, model), BF16),
            vmem((BLOCK, model), BF16),
            vmem((ways, 3 * hd, depth), BF16),
            vmem((3 * hd, depth), BF16),
            vmem((3 * hd, depth), BF16),
            vmem((2, 3 * hd, depth), BF16),
            vmem((2, 3 * hd, depth), BF16),
            vmem((3 * hd, depth), BF16),
            vmem((3 * hd, depth), BF16),
            vmem((8, BLOCK), F32),
            vmem((8, BLOCK), F32),
            vmem((BLOCK, BLOCK), F32),
            vmem((BLOCK, hd), F32),
            vmem((BLOCK, hd), F32),
            vmem((1, hd), F32),
            vmem((hd, hd), F32),
            vmem((hd, hd), F32),
            pltpu.SemaphoreType.DMA((COPIES,)),
            pltpu.SemaphoreType.DMA((COPIES + 7,)),
            pltpu.SemaphoreType.DMA((16,)),
            pltpu.SemaphoreType.DMA,
            pltpu.SemaphoreType.DMA((3,)),
        ],
        compiler_params=pltpu.CompilerParams(has_side_effects=True, vmem_limit_bytes=60 * 1024 * 1024),
    )(decay_log, hidden_in, mix_cotangent, query_weight, key_weight, value_weight)


def solution(mesh):
    placed = (
        P("dp", "sp", None),
        P("dp", "sp", None),
        P("dp", "sp"),
        P("dp", "sp"),
        P("dp", "sp"),
        P("sp"),
    )
    return jax.shard_map(
        body,
        mesh=mesh,
        in_specs=placed,
        out_specs=(P("dp", "sp", None), P("dp", "sp"), P("dp", "sp"), P("dp", "sp")),
        check_vma=False,
    )
```

time: 250 us -> 144 us (0.58)
  waiting for transfers between devices: 125 us -> 0 us
  Pallas kernels: 14.5 us -> 138 us
  blocking collectives: 42.4 us -> 0 us
  matrix products: 31.6 us -> 0 us
  between operations: 14.5 us -> 1.3 us
  starting transfers between devices: 8.54 us -> 0 us
  local copies, waits for them, and re-layouts: 10.3 us -> 4.72 us
    pallas_call x1, Pallas kernels: 14.5 us -> 138 us  [body(): pl.pallas_call(kernel, out_shape=(jax.ShapeDtypeStruct(hidden_in.shape, B...]
    all_gather x2 -> x0, waiting for transfers between devices: 96.8 us -> none  [the longest x1 73.5 us: body(): all_rows = lax.all_gather(own_rows, 'sp', axis=0, tiled=True)]
    all_to_all x1 -> x0, blocking collectives: 42.4 us -> none  [sent_and_summed(): lax.all_to_all(pieces, axis, split_axis=0, concat_axis=0, tiled=True)]
    dot_general x3 -> x0, matrix products: 31.6 us -> none  [the longest x1 11.3 us: body(): lax.dot_general(gradients, weights, (((1,), (1,)), ((), ())), preferred_e...]
    reduce_scatter x1 -> x0, waiting for transfers between devices: 27.8 us -> none  [body(): lax.psum_scatter(lax.dot_general(gradients, weights, (((1,), (1,)), ((),...]
    all_to_all x1 -> x0, starting transfers between devices: 8.42 us -> none  [body(): lax.all_to_all(mix_cotangent[0], 'sp', split_axis=1, concat_axis=0, tiled...]
    unnamed x13 -> x10, local copies, waits for them, and re-layouts: 8.72 us -> 4.72 us
  transfers between devices with their start and end apart: 4 -> 0, of which waited for: 3 -> 0; matrix products, arithmetic and copies ran while one was open for 10% -> 0% of each run, Pallas kernels for 0% -> 0%
where the time goes in v2:
time: 144 us
  Pallas kernels  138 us (96%)
  local copies, waits for them, and re-layouts  4.72 us (3%)
    pallas_call x1, Pallas kernels, body(): pl.pallas_call(kernel, out_shape=(jax.ShapeDtypeStruct(hidden_in.shape, B...  138 us
    unnamed x10, local copies, waits for them, and re-layouts  4.72 us

profile of v2, /device:TPU:1, one launch (start us, length us, event | category | flops | bytes accessed | tf_op | source)
XLA Modules:
  0.0 144.2 jit_solution(934803948613586976)
XLA Ops:
  1.3 138.2 %shard_map.93 = (bf16[1,128,2048]{2,1,0:T(8,128)(2,1)}, f32[256,256]{1,0:T(8,128)}, f32[256,256]{1,0:T(8,128)}, f32[256,256]{1,0:T(8,128)}) custom-call(f32[1]{0:T(128)S(6)} %copy.14.rate_ref, bf16[1,128,2048]{2,1,0:T(8,128)(2,1)} %hid.1, bf16[1,128,4096]{2,1,0:T(8,128)(2,1)} %cot.1, bf16[256,256]{1,0:T(8,128)(2,1)} %wq.1, bf16[256,256]{1,0:T(8,128)(2,1)} %wk.1, ...), custom_call_target="tpu_custom_call" | custom-call | tf_op jit(solution)/shard_map/pallas_call | solution.py:529
  139.5 0.0 copy-start.2
  139.5 1.9 %copy.15 = bf16[1,128,2048]{2,1,0:T(8,128)(2,1)} copy(bf16[1,128,2048]{2,1,0:T(8,128)(2,1)} %get-tuple-element.8) | data formatting | bytes 1048576
  141.4 0.0 copy-done.2
  141.4 0.0 copy-start.1
  141.4 0.7 copy.16
  142.1 0.3 copy-done.1
  142.5 0.0 copy-start
  142.5 0.7 copy.17
  143.2 0.3 copy-done
  143.5 0.7 copy.18
Async XLA Ops:
  139.5 1.9 %copy-start.2 = (f32[256,256]{1,0:T(8,128)S(1)}, f32[256,256]{1,0:T(8,128)}, u32[]{:S(2)}) copy-start(f32[256,256]{1,0:T(8,128)} %get-tuple-element.9) | copy-start | bytes 786436
  141.4 1.0 copy-start.1
  142.5 1.0 copy-start

commit v3 on v2

--- a/solution.py
+++ b/solution.py
@@ -76,12 +76,13 @@
     xr, zr = pl.ds(0, half), pl.ds(half, half)
 
     def blk(zz, xx, rows):
-        return X.at[2 * at(zz, xx) + r, rows]
+        return X.at[8 * r + at(zz, xx), rows]
 
     def ring(name, device, src):
         add(name, src, src, device)
 
-    add("swap_x", hid.at[0], X.at[2 * at(z, 3 - x) + 1], dev(swap, y * 2 + 1 - c))
+    for n, rows in enumerate((xr, zr)):
+        add("swap_x%d" % n, hid.at[0, rows], X.at[8 + at(z, 3 - x), rows], dev(swap, y * 2 + 1 - c))
     ring("A", pair, blk(z, x, xr))
     for tag, xx, rows, o in (("z", x, zr, half), ("a", x, xr, 0), ("b", xp, xr, 0)):
         ring(tag + "u", zup, blk(z, xx, rows))
@@ -92,7 +93,7 @@
         ring(tag, pair, blk(zz, x, zr))
     order = [(z, x), (down, x), (up, x), (far, x), (z, xp), (down, xp), (up, xp), (far, xp)]
     for n, (zz, xx) in enumerate(order):
-        slot = X.at[2 * at(zz, xx) + r]
+        slot = X.at[8 * r + at(zz, xx)]
         add("D%d" % n, slot, slot, sibling)
 
     for n, w in enumerate((wq, wk, wv)):
@@ -109,9 +110,9 @@
     def out(zz, xx, rows):
         return RB.at[at(zz, xx), rows]
 
-    porder = [(far, xp), (far, x), (up, xp), (up, x), (down, xp), (down, x), (z, xp), (z, x)]
-    for n, (zz, xx) in enumerate(porder):
-        add("P%d" % n, PX.at[2 * at(zz, xx) + 1 - r], RB.at[at(zz, xx)], sibling)
+    zorder = (far, up, down, z)
+    for n, zz in enumerate(zorder):
+        add("P%d" % n, PX.at[pl.ds(8 * (1 - r) + 2 * zz, 2)], RB.at[pl.ds(2 * zz, 2)], sibling)
     for n, zz in enumerate((far, up, down, z)):
         add("EZ%d" % n, out(zz, xp, zr), EZ.at[zz], pair)
     cols3 = ((0, x, 0), (1, xp, 0), (2, x, half))
@@ -132,37 +133,37 @@
         add("hb1_%d" % i, DW.at[2 * y + i], HB1, dev(swap, 2 * y + i), COPIES + 6)
     add("hb0", DW.at[2 * y + 1 - c], HB0, sibling)
 
+    barrier = pltpu.get_barrier_semaphore()
+
+    def greet(k, _):
+        pl.semaphore_signal(
+            barrier, inc=1, device_id=dev((s + k // 2) % 16, 2 * y + (c + k) % 2),
+            device_id_type=pl.DeviceIdType.MESH,
+        )
+        return 0
+
+    for device in (yup, ydown):
+        pl.semaphore_signal(barrier, inc=1, device_id=device, device_id_type=pl.DeviceIdType.MESH)
+    lax.fori_loop(1, 32, greet, 0)
+
+    def local_weights():
+        return [
+            pltpu.make_async_copy(w, W.at[d, :, pl.ds(n * hd, hd)], lsem.at[n])
+            for n, w in enumerate((wq, wk, wv))
+        ]
+
+    @pl.when(r == 0)
+    def _():
+        for n, rows in enumerate((xr, zr)):
+            pltpu.make_async_copy(hid.at[0, rows], X.at[j, rows], rs.at[n]).start()
+        for copy in local_weights():
+            copy.start()
+
     RT[...] = jnp.full(RT.shape, rate_ref[0], F32)
-
-    own_x = X.at[2 * j + r]
-    local_x = pltpu.make_async_copy(hid.at[0], X.at[2 * j], rs.at[0])
-
-    @pl.when(r == 0)
-    def _():
-        local_x.start()
-
-    @pl.when(r == 1)
-    def _():
-        start("swap_x")
-
-    for n, w in enumerate((wq, wk, wv)):
-        start("swap_w%d" % n)
-
-    @pl.when(r == 0)
-    def _():
-        for n, w in enumerate((wq, wk, wv)):
-            pltpu.make_async_copy(w, W.at[d, :, pl.ds(n * hd, hd)], lsem.at[n]).start()
-
-    @pl.when(r == 1)
-    def _():
-        for n in range(3):
-            start("own_w%d" % n)
-
-    pltpu.make_async_copy(own_x, own_x, rs.at[0]).wait()
-    start("A", "zu", "zd", "H0", "au", "ad", "D0")
+    pl.semaphore_wait(barrier, 33)
 
     bx = x + r * (3 - 2 * x)
-    cslot = 2 * (z * 2 + bx - 2 * c) + r
+    cslot = 8 * r + z * 2 + bx - 2 * c
 
     def cot_copy(k):
         h = (s + k) % 16
@@ -190,17 +191,49 @@
 
         return 0
 
-    lax.fori_loop(0, 16, cot_send, 0)
+    def wait_own(n, rows):
+        own = X.at[8 * r + j, rows]
+        pltpu.make_async_copy(own, own, rs.at[n]).wait()
+
+    def late_a():
+        arrived("H1")
+        start("D5")
+        arrived("H2")
+        start("D6")
+
+    def late_b():
+        arrived("buu", "bdd", "H3")
+        start("D7")
+
+    @pl.when(r == 1)
+    def _():
+        start("swap_x0", "swap_x1")
+        for n in range(3):
+            start("own_w%d" % n)
+        for n in range(3):
+            start("swap_w%d" % n)
+        lax.fori_loop(0, 16, cot_send, 0)
+
+    wait_own(0, xr)
+    start("A", "au", "ad")
+    wait_own(1, zr)
+    start("zu", "zd", "H0", "D0")
+
+    @pl.when(r == 0)
+    def _():
+        for copy in local_weights():
+            copy.wait()
+        arrived("own_w0", "own_w1", "own_w2")
+        start("wu0", "wd1", "wu1", "wd0")
+
     start("rate")
-
     arrived("A")
     start("bu", "bd")
 
     @pl.when(r == 0)
     def _():
-        for n, w in enumerate((wq, wk, wv)):
-            pltpu.make_async_copy(w, W.at[d, :, pl.ds(n * hd, hd)], lsem.at[n]).wait()
-        arrived("own_w0", "own_w1", "own_w2")
+        for n in range(3):
+            start("swap_w%d" % n)
 
     @pl.when(r == 1)
     def _():
@@ -208,56 +241,73 @@
             for i in range(2):
                 piece = W.at[2 * y + i, :, pl.ds(n * hd, hd)]
                 pltpu.make_async_copy(piece, piece, rs.at[COPIES + 2 * n + i]).wait()
-
-    start("wu0", "wd1", "wu1", "wd0")
-
+        start("wu0", "wd1", "wu1", "wd0")
+
+    arrived("au")
+    start("auu")
+    arrived("ad")
+    start("add")
     arrived("zu")
-    start("zuu", "H1")
+    start("zuu", "H1", "D1")
     arrived("zd")
-    start("zdd", "H2")
-    arrived("au")
-    start("auu", "D1")
-    arrived("ad")
-    start("add", "D2")
+    start("zdd", "H2", "D2")
+
+    def forward_weights():
+        arrived("wu0")
+        start("wuu")
+        arrived("wd1")
+        start("wdd")
+
+    @pl.when(r == 0)
+    def _():
+        forward_weights()
+
     arrived("bu")
     start("buu")
     arrived("bd")
     start("bdd")
+
+    @pl.when(r == 0)
+    def _():
+        lax.fori_loop(0, 16, cot_send, 0)
+
     arrived("zuu", "zdd")
     start("H3")
-    arrived("wu0")
-    start("wuu")
-    arrived("wd1")
-    start("wdd")
+
+    @pl.when(r == 1)
+    def _():
+        forward_weights()
+
     arrived("auu", "add")
     start("D3")
     arrived("H0")
     start("D4")
+
+    @pl.when(r == 0)
+    def _():
+        late_a()
+        late_b()
+
     arrived("wu1", "wd0", "wuu", "wdd")
 
     def project(k, _):
-        @pl.when(k == 3)
-        def _():
-            arrived("H1")
-            start("D5")
-            arrived("H2")
-            start("D6")
-
-        @pl.when(k == 6)
-        def _():
-            arrived("buu", "bdd", "H3")
-            start("D7")
-
-        for n in range(8):
-
-            @pl.when(k == n)
+        @pl.when(jnp.logical_and(r == 1, k == 4))
+        def _():
+            late_a()
+
+        @pl.when(jnp.logical_and(r == 1, k == 6))
+        def _():
+            late_b()
+
+        for n in range(4):
+
+            @pl.when(k == n + 4 * (1 - r))
             def _():
-                arrived("D%d" % n)
+                arrived("D%d" % n, "D%d" % (n + 4))
 
         q = k % 4
         zz = (z + jnp.where(q == 0, 0, jnp.where(q == 1, 3, jnp.where(q == 2, 1, 2)))) % 4
-        jj = at(zz, x + k // 4)
-        rows = pl.ds(2 * jj, 2)
+        rows = pl.ds(8 * (k // 4) + 2 * zz, 2)
         a = X[rows].reshape(2 * BLOCK, X.shape[2])
         for n in range(3):
             b = W[:, :, n * hd : (n + 1) * hd].reshape(X.shape[2], hd)
@@ -287,7 +337,7 @@
     def load(n):
         px = n % 4
         role = (px // 2 + g) % 2
-        slot = 2 * at(n // 4, px + role * (3 - 2 * px)) + role
+        slot = 8 * role + at(n // 4, px + role * (3 - 2 * px))
         q = QKV[slot, :, 0:hd]
         k = (QKV[slot, :, hd : 2 * hd].astype(F32) * scale).astype(BF16)
         v = QKV[slot, :, 2 * hd : 3 * hd]
@@ -321,10 +371,14 @@
     lax.fori_loop(0, blocks, retain, 0)
 
     def chip_sum(n):
-        zz, xx = porder[n]
+        zz = zorder[n]
         arrived("P%d" % n)
-        jj = at(zz, xx)
-        RB[jj] = both(RB[jj], PX[2 * jj + r])
+        for xx, names in ((xp, ("EZ%d" % n, "FU1", "FD1")), (x, ("FU0", "FD0"))):
+            jj = at(zz, xx)
+            RB[jj] = both(RB[jj], PX[8 * r + jj])
+            if n:
+                names = tuple(name for name in names if name[0] == "E")
+            start(*names)
 
     def merge(ref, index, rows, other):
         ref[index, rows] = both(ref[index, rows], other)
@@ -351,19 +405,7 @@
         i = jnp.where(jnp.logical_or(k == 2, k == 3), (k + 1) % 2, k % 2)
         return 2 * ((y + yo) % 4) + i
 
-    def products(k, _):
-        jj = at((z + offset(k // 2)) % 4, x + 1 - k % 2)
-        rows = pl.ds(2 * jj, 2)
-        a = G[rows].reshape(2 * BLOCK, 3 * hd)
-        for n in range(8):
-            piece = dot(a, W[n], (1, 1)).astype(BF16)
-            PX[rows, :, n * depth : (n + 1) * depth] = piece.reshape(2, BLOCK, depth)
-        for n in range(8):
-
-            @pl.when(k == n)
-            def _():
-                start("P%d" % n)
-
+    def weights_product(k):
         db = yblock(k)
         cols = pl.ds(pl.multiple_of(db * depth, depth), depth)
         b = X[:, :, cols].reshape(blocks * BLOCK, depth)
@@ -371,71 +413,75 @@
             part = pl.ds(n * hd, hd)
             DW[db, part, :] = dot(GT[part, :], b, (1, 0)).astype(BF16)
 
-        @pl.when(k == 0)
-        def _():
-            start("YFU")
-            chip_sum(0)
-            start("EZ0", "FU1", "FD1")
-
-        @pl.when(k == 1)
-        def _():
-            start("YFD")
-            chip_sum(1)
-            start("FU0", "FD0")
-
-        @pl.when(k == 2)
-        def _():
-            start("YSU1")
-            chip_sum(2)
-            start("EZ1")
-
-        @pl.when(k == 3)
-        def _():
-            start("YSD0")
-            chip_sum(3)
+    def products(k, _):
+        weights_product(k)
+        for n, names in enumerate((("YFU",), ("YFD",), ("YSU1",), ("YSD0",))):
+
+            @pl.when(k == n)
+            def _():
+                start(*names)
+
+        q = k // 2
+        zz = (z + offset(q)) % 4
+        rows = pl.ds(8 * ((1 - r + k) % 2) + 2 * zz, 2)
+        a = G[rows].reshape(2 * BLOCK, 3 * hd)
+        for n in range(8):
+            piece = dot(a, W[n], (1, 1)).astype(BF16)
+            PX[rows, :, n * depth : (n + 1) * depth] = piece.reshape(2, BLOCK, depth)
+        for n in range(4):
+
+            @pl.when(k == 2 * n)
+            def _():
+                start("P%d" % n)
+
+            @pl.when(k == 2 * n + 1)
+            def _():
+                chip_sum(n)
+
+        @pl.when(k == 4)
+        def _():
             ring_up(1)
-
-        @pl.when(k == 4)
-        def _():
-            chip_sum(4)
-            start("EZ2")
+            ring_up(0)
+            arrived("YFU")
+            DW[2 * yu] = both(DW[2 * yu], YFU[...])
+            start("YSU0")
+
+        @pl.when(k == 5)
+        def _():
             ring_down(1)
-            ring_up(0)
-
-        @pl.when(k == 5)
-        def _():
-            chip_sum(5)
             ring_down(0)
             pair_in(0)
             start("FU2", "FD2")
-            arrived("YFU")
-            DW[2 * yu] = both(DW[2 * yu], YFU[...])
-            start("YSU0")
-
-        @pl.when(k == 6)
-        def _():
             arrived("YFD")
             DW[2 * yd + 1] = both(DW[2 * yd + 1], YFD[...])
             start("YSD1")
-            chip_sum(6)
-            start("EZ3")
-            pair_in(1)
-            ring_up(2)
-
-        @pl.when(k == 7)
-        def _():
-            chip_sum(7)
-            pair_in(2)
-            ring_down(2)
 
         return 0
 
     lax.fori_loop(0, 8, products, 0)
 
+    jp = at(z, xp)
     arrived("SU1", "SD1")
-    jp = at(z, xp)
     RB[jp, xr] = (RB[jp, xr].astype(F32) + SU[1].astype(F32) + SD[1].astype(F32)).astype(BF16)
     start("EX")
+    pair_in(1)
+    ring_up(2)
+    pair_in(2)
+    ring_down(2)
+
+    for i in range(2):
+        arrived("YSU%d" % i, "YSD%d" % i)
+        total = DW[2 * y + i].astype(F32) + YSU[i].astype(F32) + YSD[i].astype(F32)
+        DW[2 * y + i] = total.astype(BF16)
+
+        @pl.when(r == 1)
+        def _():
+            start("hb1_%d" % i)
+
+    @pl.when(r == 0)
+    def _():
+        start("hb0")
+
     arrived("SU0", "SD0", "EX")
     total = RB[j, xr].astype(F32) + SU[0].astype(F32) + SD[0].astype(F32) + EX[...].astype(F32)
     FIN[xr] = total.astype(BF16)
@@ -443,19 +489,6 @@
     @pl.when(r == 1)
     def _():
         start("fin0")
-
-    arrived("YSU1", "YSD0", "YSU0", "YSD1")
-    for i in range(2):
-        total = DW[2 * y + i].astype(F32) + YSU[i].astype(F32) + YSD[i].astype(F32)
-        DW[2 * y + i] = total.astype(BF16)
-
-    @pl.when(r == 0)
-    def _():
-        start("hb0")
-
-    @pl.when(r == 1)
-    def _():
-        start("hb1_0", "hb1_1")
 
     pair_in(3)
     arrived("SU2", "SD2")
@@ -488,7 +521,7 @@
         arrived("fin0", "fin1")
         dx_out[0] = RFIN[...]
 
-    only_one = ("swap_x", "own_w0", "own_w1", "own_w2", "fin0", "fin1", "hb1_0", "hb1_1")
+    only_one = ("swap_x0", "swap_x1", "own_w0", "own_w1", "own_w2", "fin0", "fin1", "hb1_0", "hb1_1")
     for name in copies:
         if name not in only_one and name != "hb0":
             copies[name].wait_send()
@@ -515,6 +548,15 @@
         return 0
 
     lax.fori_loop(0, 16, cot_done, 0)
+
+
+def hand_over(*refs):
+    n = len(refs) // 2
+    pairs = [pltpu.make_async_copy(refs[i], refs[n + i], refs[-1].at[i]) for i in range(n)]
+    for copy in pairs:
+        copy.start()
+    for copy in pairs:
+        copy.wait()
 
 
 def body(hidden_in, mix_cotangent, query_weight, key_weight, value_weight, decay_log):
@@ -524,12 +566,13 @@
     slots = 16
     vmem = pltpu.VMEM
     any_space = pl.BlockSpec(memory_space=pl.ANY)
+    far_space = pl.BlockSpec(memory_space=pltpu.HBM)
     whole = pl.BlockSpec(memory_space=pltpu.VMEM)
     grad = jax.ShapeDtypeStruct((depth, hd), F32)
-    return pl.pallas_call(
+    results = pl.pallas_call(
         kernel,
         out_shape=(jax.ShapeDtypeStruct(hidden_in.shape, BF16), grad, grad, grad),
-        in_specs=[pl.BlockSpec(memory_space=pltpu.SMEM)] + [any_space] * 5,
+        in_specs=[pl.BlockSpec(memory_space=pltpu.SMEM)] + [far_space] * 5,
         out_specs=(whole,) * 4,
         scratch_shapes=[
             vmem((slots, BLOCK, model), BF16),
@@ -569,8 +612,16 @@
             pltpu.SemaphoreType.DMA,
             pltpu.SemaphoreType.DMA((3,)),
         ],
-        compiler_params=pltpu.CompilerParams(has_side_effects=True, vmem_limit_bytes=60 * 1024 * 1024),
+        compiler_params=pltpu.CompilerParams(collective_id=0, has_side_effects=True, vmem_limit_bytes=52 * 1024 * 1024),
     )(decay_log, hidden_in, mix_cotangent, query_weight, key_weight, value_weight)
+    return pl.pallas_call(
+        hand_over,
+        out_shape=(jax.ShapeDtypeStruct(hidden_in.shape, BF16), grad, grad, grad),
+        in_specs=[any_space] * 4,
+        out_specs=(any_space,) * 4,
+        scratch_shapes=[pltpu.SemaphoreType.DMA((4,))],
+        compiler_params=pltpu.CompilerParams(vmem_limit_bytes=1024 * 1024),
+    )(*results)
 
 
 def solution(mesh):

time: 144 us -> 129 us (0.90)
  Pallas kernels: 138 us -> 125 us
  local copies, waits for them, and re-layouts: 4.72 us -> 2.7 us
    pallas_call x1, Pallas kernels: 138 us -> 124 us  [body(): pl.pallas_call(kernel, out_shape=(jax.ShapeDtypeStruct(hidden_in.shape, B...]
    unnamed x10 -> x6, local copies, waits for them, and re-layouts: 4.72 us -> 2.7 us
where the time goes in v3:
time: 129 us
  Pallas kernels  125 us (97%)
  local copies, waits for them, and re-layouts  2.7 us (2%)
  between operations  1.3 us (1%)
    pallas_call x1, Pallas kernels, body(): pl.pallas_call(kernel, out_shape=(jax.ShapeDtypeStruct(hidden_in.shape, B...  124 us
    unnamed x6, local copies, waits for them, and re-layouts  2.7 us

profile of v3, /device:TPU:1, one launch (start us, length us, event | category | flops | bytes accessed | tf_op | source)
XLA Modules:
  0.0 128.7 jit_solution(7328084271170025344)
XLA Ops:
  1.3 0.0 copy-start
  1.3 0.9 copy-done
  2.2 0.0 copy-start.1
  2.2 0.9 copy-done.1
  3.1 0.0 copy-start.2
  3.1 0.9 copy-done.2
  4.0 123.6 %shard_map.93 = (bf16[1,128,2048]{2,1,0:T(8,128)(2,1)S(1)}, f32[256,256]{1,0:T(8,128)S(1)}, f32[256,256]{1,0:T(8,128)S(1)}, f32[256,256]{1,0:T(8,128)S(1)}) custom-call(f32[1]{0:T(128)S(6)} %copy.10.rate_ref, bf16[1,128,2048]{2,1,0:T(8,128)(2,1)} %hid.1, bf16[1,128,4096]{2,1,0:T(8,128)(2,1)} %cot.1, bf16[256,256]{1,0:T(8,128)(2,1)S(1)} %copy-done, ...), custom_call_target="tpu_custom_call" | custom-call | tf_op jit(solution)/shard_map/pallas_call | solution.py:572
  127.6 1.1 shard_map.94
Async XLA Ops:
  1.3 0.9 copy-start
  2.2 0.9 copy-start.1
  3.1 0.9 copy-start.2

commit v4 on v3

--- a/solution.py
+++ b/solution.py
@@ -6,7 +6,7 @@
 from jax.sharding import PartitionSpec as P
 
 BLOCK = 128
-COPIES = 96
+COPIES = 128
 BF16 = jnp.bfloat16
 F32 = jnp.float32
 
@@ -24,14 +24,14 @@
 
 
 def kernel(
-    rate_ref, hid, cot, wq, wk, wv,
+    rate_ref, hid, cot, wall,
     dx_out, dq_out, dk_out, dv_out,
     X, W, C, QKV, G, GT, PX, RB, EZ, FU, FD, SU, SD, EX, FIN, RFIN,
     DW, YFU, YFD, YSU, YSD, HB0, HB1, RT, PR, inner, qdec, kdec, sdec, fstate, bstate,
     ss, rs, csend, crecv, lsem,
 ):
-    hd = wq.shape[1]
-    depth = wq.shape[0]
+    depth = wall.shape[0]
+    hd = wall.shape[1] // 3
     s = lax.axis_index("sp")
     d = lax.axis_index("dp")
     z, x = s // 4, s % 4
@@ -96,10 +96,8 @@
         slot = X.at[8 * r + at(zz, xx)]
         add("D%d" % n, slot, slot, sibling)
 
-    for n, w in enumerate((wq, wk, wv)):
-        cols = pl.ds(n * hd, hd)
-        add("own_w%d" % n, w, W.at[d, :, cols], sibling)
-        add("swap_w%d" % n, w, W.at[d, :, cols], dev(swap, y * 2 + g), COPIES + 2 * n + c)
+    add("own_w", wall, W.at[d], sibling)
+    add("swap_w", wall, W.at[d], dev(swap, y * 2 + g), COPIES + c)
     for i in range(2):
         ring("wu%d" % i, yup, W.at[2 * y + i])
         ring("wd%d" % i, ydown, W.at[2 * y + i])
@@ -125,13 +123,17 @@
     for n, rows in enumerate((xr, zr)):
         add("fin%d" % n, FIN.at[rows], RFIN.at[rows], dev(swap, y * 2 + 1 - c))
 
-    add("YFU", DW.at[2 * yf], YFU, yup)
-    add("YFD", DW.at[2 * yf + 1], YFD, ydown)
-    for i in range(2):
-        add("YSU%d" % i, DW.at[2 * yu + i], YSU.at[i], yup)
-        add("YSD%d" % i, DW.at[2 * yd + i], YSD.at[i], ydown)
-        add("hb1_%d" % i, DW.at[2 * y + i], HB1, dev(swap, 2 * y + i), COPIES + 6)
-    add("hb0", DW.at[2 * y + 1 - c], HB0, sibling)
+    for n in range(3):
+        add("YFU_%d" % n, DW.at[n, 2 * yf], YFU.at[n], yup)
+        add("YFD_%d" % n, DW.at[n, 2 * yf + 1], YFD.at[n], ydown)
+        for i in range(2):
+            add("YSU%d_%d" % (i, n), DW.at[n, 2 * yu + i], YSU.at[n, i], yup)
+            add("YSD%d_%d" % (i, n), DW.at[n, 2 * yd + i], YSD.at[n, i], ydown)
+            add("hb1_%d_%d" % (i, n), DW.at[n, 2 * y + i], HB1.at[n], dev(swap, 2 * y + i), COPIES + 2 + n)
+        add("hb0_%d" % n, DW.at[n, 2 * y + 1 - c], HB0.at[n], sibling)
+
+    def parts(name):
+        return tuple("%s_%d" % (name, n) for n in range(3))
 
     barrier = pltpu.get_barrier_semaphore()
 
@@ -146,18 +148,13 @@
         pl.semaphore_signal(barrier, inc=1, device_id=device, device_id_type=pl.DeviceIdType.MESH)
     lax.fori_loop(1, 32, greet, 0)
 
-    def local_weights():
-        return [
-            pltpu.make_async_copy(w, W.at[d, :, pl.ds(n * hd, hd)], lsem.at[n])
-            for n, w in enumerate((wq, wk, wv))
-        ]
+    local_weights = pltpu.make_async_copy(wall, W.at[d], lsem)
 
     @pl.when(r == 0)
     def _():
         for n, rows in enumerate((xr, zr)):
             pltpu.make_async_copy(hid.at[0, rows], X.at[j, rows], rs.at[n]).start()
-        for copy in local_weights():
-            copy.start()
+        local_weights.start()
 
     RT[...] = jnp.full(RT.shape, rate_ref[0], F32)
     pl.semaphore_wait(barrier, 33)
@@ -173,7 +170,7 @@
         tc = c + role * (1 - 2 * c)
         src = cot.at[0, :, pl.ds(pl.multiple_of(h * hd, hd), hd)]
         same = jnp.logical_and(r == 0, k == 0)
-        return same, src, dev(hz * 4 + tx, 2 * y + tc), csend.at[k]
+        return same, src, dev(hz * 4 + tx, 2 * y + tc), csend
 
     def cot_send(k, _):
         same, src, device, sem = cot_copy(k)
@@ -208,22 +205,22 @@
     @pl.when(r == 1)
     def _():
         start("swap_x0", "swap_x1")
-        for n in range(3):
-            start("own_w%d" % n)
-        for n in range(3):
-            start("swap_w%d" % n)
-        lax.fori_loop(0, 16, cot_send, 0)
+        start("own_w")
 
     wait_own(0, xr)
     start("A", "au", "ad")
+
+    @pl.when(r == 1)
+    def _():
+        start("swap_w")
+
     wait_own(1, zr)
     start("zu", "zd", "H0", "D0")
 
     @pl.when(r == 0)
     def _():
-        for copy in local_weights():
-            copy.wait()
-        arrived("own_w0", "own_w1", "own_w2")
+        local_weights.wait()
+        arrived("own_w")
         start("wu0", "wd1", "wu1", "wd0")
 
     start("rate")
@@ -232,15 +229,13 @@
 
     @pl.when(r == 0)
     def _():
-        for n in range(3):
-            start("swap_w%d" % n)
-
-    @pl.when(r == 1)
-    def _():
-        for n in range(3):
-            for i in range(2):
-                piece = W.at[2 * y + i, :, pl.ds(n * hd, hd)]
-                pltpu.make_async_copy(piece, piece, rs.at[COPIES + 2 * n + i]).wait()
+        start("swap_w")
+
+    @pl.when(r == 1)
+    def _():
+        for i in range(2):
+            piece = W.at[2 * y + i]
+            pltpu.make_async_copy(piece, piece, rs.at[COPIES + i]).wait()
         start("wu0", "wd1", "wu1", "wd0")
 
     arrived("au")
@@ -258,25 +253,22 @@
         arrived("wd1")
         start("wdd")
 
-    @pl.when(r == 0)
-    def _():
-        forward_weights()
+    forward_weights()
+
+    @pl.when(r == 1)
+    def _():
+        lax.fori_loop(0, 16, cot_send, 0)
 
     arrived("bu")
     start("buu")
     arrived("bd")
     start("bdd")
-
-    @pl.when(r == 0)
-    def _():
-        lax.fori_loop(0, 16, cot_send, 0)
-
     arrived("zuu", "zdd")
     start("H3")
 
-    @pl.when(r == 1)
-    def _():
-        forward_weights()
+    @pl.when(r == 0)
+    def _():
+        lax.fori_loop(0, 16, cot_send, 0)
 
     arrived("auu", "add")
     start("D3")
@@ -411,54 +403,82 @@
         b = X[:, :, cols].reshape(blocks * BLOCK, depth)
         for n in range(3):
             part = pl.ds(n * hd, hd)
-            DW[db, part, :] = dot(GT[part, :], b, (1, 0)).astype(BF16)
-
-    def products(k, _):
-        weights_product(k)
-        for n, names in enumerate((("YFU",), ("YFD",), ("YSU1",), ("YSD0",))):
-
-            @pl.when(k == n)
-            def _():
-                start(*names)
-
-        q = k // 2
-        zz = (z + offset(q)) % 4
-        rows = pl.ds(8 * ((1 - r + k) % 2) + 2 * zz, 2)
+            DW[n, db] = dot(GT[part, :], b, (1, 0)).astype(BF16)
+
+    def input_product(k, role):
+        zz = (z + offset(k)) % 4
+        rows = pl.ds(8 * role + 2 * zz, 2)
         a = G[rows].reshape(2 * BLOCK, 3 * hd)
         for n in range(8):
             piece = dot(a, W[n], (1, 1)).astype(BF16)
             PX[rows, :, n * depth : (n + 1) * depth] = piece.reshape(2, BLOCK, depth)
+
+    def products(k, _):
+        input_product(k, 1 - r)
         for n in range(4):
 
-            @pl.when(k == 2 * n)
+            @pl.when(k == n)
             def _():
                 start("P%d" % n)
 
-            @pl.when(k == 2 * n + 1)
+        input_product(k, r)
+        weights_product(2 * k)
+        for n, names in enumerate((parts("YFU"), parts("YSU1"))):
+
+            @pl.when(k == n)
+            def _():
+                start(*names)
+
+        for n in range(4):
+
+            @pl.when(k == n)
             def _():
                 chip_sum(n)
 
-        @pl.when(k == 4)
+        @pl.when(k == 2)
         def _():
             ring_up(1)
-            ring_up(0)
-            arrived("YFU")
-            DW[2 * yu] = both(DW[2 * yu], YFU[...])
-            start("YSU0")
-
-        @pl.when(k == 5)
-        def _():
             ring_down(1)
-            ring_down(0)
             pair_in(0)
             start("FU2", "FD2")
-            arrived("YFD")
-            DW[2 * yd + 1] = both(DW[2 * yd + 1], YFD[...])
-            start("YSD1")
+            ring_up(0)
+            for n in range(3):
+                arrived("YFU_%d" % n)
+                DW[n, 2 * yu] = both(DW[n, 2 * yu], YFU[n])
+                start("YSU0_%d" % n)
+
+        weights_product(2 * k + 1)
+        for n, names in enumerate((parts("YFD"), parts("YSD0"))):
+
+            @pl.when(k == n)
+            def _():
+                start(*names)
+
+        @pl.when(k == 2)
+        def _():
+            ring_down(0)
+            for n in range(3):
+                arrived("YFD_%d" % n)
+                DW[n, 2 * yd + 1] = both(DW[n, 2 * yd + 1], YFD[n])
+                start("YSD1_%d" % n)
 
         return 0
 
-    lax.fori_loop(0, 8, products, 0)
+    lax.fori_loop(0, 4, products, 0)
+
+    def weight_sums(n):
+        for i in range(2):
+            arrived("YSU%d_%d" % (i, n), "YSD%d_%d" % (i, n))
+            total = DW[n, 2 * y + i].astype(F32) + YSU[n, i].astype(F32) + YSD[n, i].astype(F32)
+            DW[n, 2 * y + i] = total.astype(BF16)
+
+        @pl.when(r == 1)
+        def _():
+            start("hb1_0_%d" % n, "hb1_1_%d" % n)
+
+        @pl.when(r == 0)
+        def _():
+            start("hb0_%d" % n)
 
     jp = at(z, xp)
     arrived("SU1", "SD1")
@@ -466,22 +486,11 @@
     start("EX")
     pair_in(1)
     ring_up(2)
+    weight_sums(0)
     pair_in(2)
     ring_down(2)
-
-    for i in range(2):
-        arrived("YSU%d" % i, "YSD%d" % i)
-        total = DW[2 * y + i].astype(F32) + YSU[i].astype(F32) + YSD[i].astype(F32)
-        DW[2 * y + i] = total.astype(BF16)
-
-        @pl.when(r == 1)
-        def _():
-            start("hb1_%d" % i)
-
-    @pl.when(r == 0)
-    def _():
-        start("hb0")
-
+    weight_sums(1)
+    weight_sums(2)
     arrived("SU0", "SD0", "EX")
     total = RB[j, xr].astype(F32) + SU[0].astype(F32) + SD[0].astype(F32) + EX[...].astype(F32)
     FIN[xr] = total.astype(BF16)
@@ -503,27 +512,26 @@
     def _():
         start("fin1")
 
-    copies["hb1_0"].wait_recv()
-
-    def weights_out(part):
-        for n, ref in enumerate((dq_out, dk_out, dv_out)):
-            rows = pl.ds(n * hd, hd)
-            ref[...] = ((part[rows].astype(F32) + HB1[rows].astype(F32)) * 0.125).T
-
-    @pl.when(r == 0)
-    def _():
-        weights_out(DW.at[2 * y + c])
-
-    @pl.when(r == 1)
-    def _():
-        arrived("hb0")
-        weights_out(HB0)
+    for n, ref in enumerate((dq_out, dk_out, dv_out)):
+        pltpu.make_async_copy(HB1.at[n], HB1.at[n], rs.at[COPIES + 2 + n]).wait()
+
+        @pl.when(r == 0)
+        def _():
+            ref[...] = ((DW[n, 2 * y + c].astype(F32) + HB1[n].astype(F32)) * 0.125).T
+
+        @pl.when(r == 1)
+        def _():
+            arrived("hb0_%d" % n)
+            ref[...] = ((HB0[n].astype(F32) + HB1[n].astype(F32)) * 0.125).T
+
+    @pl.when(r == 1)
+    def _():
         arrived("fin0", "fin1")
         dx_out[0] = RFIN[...]
 
-    only_one = ("swap_x0", "swap_x1", "own_w0", "own_w1", "own_w2", "fin0", "fin1", "hb1_0", "hb1_1")
+    only_one = ("swap_x0", "swap_x1", "own_w", "fin0", "fin1") + parts("hb1_0") + parts("hb1_1")
     for name in copies:
-        if name not in only_one and name != "hb0":
+        if name not in only_one and name[:3] != "hb0":
             copies[name].wait_send()
 
     @pl.when(r == 1)
@@ -533,21 +541,15 @@
 
     @pl.when(r == 0)
     def _():
-        copies["hb0"].wait_send()
-
-    def cot_done(k, _):
-        same, src, device, sem = cot_copy(k)
-
-        @pl.when(jnp.logical_not(same))
-        def _():
-            pltpu.make_async_remote_copy(
-                src_ref=src, dst_ref=C.at[cslot], send_sem=sem, recv_sem=crecv,
-                device_id=device, device_id_type=pl.DeviceIdType.MESH,
-            ).wait_send()
-
-        return 0
-
-    lax.fori_loop(0, 16, cot_done, 0)
+        for name in parts("hb0"):
+            copies[name].wait_send()
+
+    for role in range(2):
+
+        @pl.when(r == role)
+        def _():
+            sent = C.at[pl.ds(0, 15 + role)]
+            pltpu.make_async_copy(sent, sent, csend).wait()
 
 
 def hand_over(*refs):
@@ -569,10 +571,11 @@
     far_space = pl.BlockSpec(memory_space=pltpu.HBM)
     whole = pl.BlockSpec(memory_space=pltpu.VMEM)
     grad = jax.ShapeDtypeStruct((depth, hd), F32)
+    weights = jnp.concatenate((query_weight, key_weight, value_weight), axis=1)
     results = pl.pallas_call(
         kernel,
         out_shape=(jax.ShapeDtypeStruct(hidden_in.shape, BF16), grad, grad, grad),
-        in_specs=[pl.BlockSpec(memory_space=pltpu.SMEM)] + [far_space] * 5,
+        in_specs=[pl.BlockSpec(memory_space=pltpu.SMEM)] + [far_space] * 3,
         out_specs=(whole,) * 4,
         scratch_shapes=[
             vmem((slots, BLOCK, model), BF16),
@@ -591,13 +594,13 @@
             vmem((BLOCK // 2, model), BF16),
             vmem((BLOCK, model), BF16),
             vmem((BLOCK, model), BF16),
-            vmem((ways, 3 * hd, depth), BF16),
-            vmem((3 * hd, depth), BF16),
-            vmem((3 * hd, depth), BF16),
-            vmem((2, 3 * hd, depth), BF16),
-            vmem((2, 3 * hd, depth), BF16),
-            vmem((3 * hd, depth), BF16),
-            vmem((3 * hd, depth), BF16),
+            vmem((3, ways, hd, depth), BF16),
+            vmem((3, hd, depth), BF16),
+            vmem((3, hd, depth), BF16),
+            vmem((3, 2, hd, depth), BF16),
+            vmem((3, 2, hd, depth), BF16),
+            vmem((3, hd, depth), BF16),
+            vmem((3, hd, depth), BF16),
             vmem((8, BLOCK), F32),
             vmem((8, BLOCK), F32),
             vmem((BLOCK, BLOCK), F32),
@@ -607,13 +610,13 @@
             vmem((hd, hd), F32),
             vmem((hd, hd), F32),
             pltpu.SemaphoreType.DMA((COPIES,)),
-            pltpu.SemaphoreType.DMA((COPIES + 7,)),
-            pltpu.SemaphoreType.DMA((16,)),
+            pltpu.SemaphoreType.DMA((COPIES + 5,)),
             pltpu.SemaphoreType.DMA,
-            pltpu.SemaphoreType.DMA((3,)),
+            pltpu.SemaphoreType.DMA,
+            pltpu.SemaphoreType.DMA,
         ],
         compiler_params=pltpu.CompilerParams(collective_id=0, has_side_effects=True, vmem_limit_bytes=52 * 1024 * 1024),
-    )(decay_log, hidden_in, mix_cotangent, query_weight, key_weight, value_weight)
+    )(decay_log, hidden_in, mix_cotangent, weights)
     return pl.pallas_call(
         hand_over,
         out_shape=(jax.ShapeDtypeStruct(hidden_in.shape, BF16), grad, grad, grad),

time: 129 us -> 114 us (0.88)
  Pallas kernels: 125 us -> 111 us
  local copies, waits for them, and re-layouts: 2.7 us -> 0 us
    pallas_call x1, Pallas kernels: 124 us -> 110 us  [body(): pl.pallas_call(kernel, out_shape=(jax.ShapeDtypeStruct(hidden_in.shape, B...]
    unnamed x6 -> x0, local copies, waits for them, and re-layouts: 2.7 us -> none
where the time goes in v4:
time: 114 us
  Pallas kernels  111 us (97%)
  between operations  1.29 us (1%)
    pallas_call x1, Pallas kernels, body(): pl.pallas_call(kernel, out_shape=(jax.ShapeDtypeStruct(hidden_in.shape, B...  110 us

profile of v4, /device:TPU:1, one launch (start us, length us, event | category | flops | bytes accessed | tf_op | source)
XLA Modules:
  0.0 113.8 jit_solution(2256380026748086890)
XLA Ops:
  1.3 1.1 pad_maximum_fusion.wall
  2.3 110.3 %shard_map.93 = (bf16[1,128,2048]{2,1,0:T(8,128)(2,1)S(1)}, f32[256,256]{1,0:T(8,128)S(1)}, f32[256,256]{1,0:T(8,128)S(1)}, f32[256,256]{1,0:T(8,128)S(1)}) custom-call(f32[1]{0:T(128)S(6)} %copy.10.rate_ref, bf16[1,128,2048]{2,1,0:T(8,128)(2,1)} %hid.1, bf16[1,128,4096]{2,1,0:T(8,128)(2,1)} %cot.1, bf16[256,768]{1,0:T(8,128)(2,1)S(1)} %pad_maximum_fusion.wall), custom_call_target="tpu_custom_call" | custom-call | tf_op jit(solution)/shard_map/pallas_call | solution.py:575
  112.7 1.1 shard_map.94
